TPU v7x, 512 devices: a whole 4x8x8 slice. The times are simulated.
512 devices in a mesh: ep: 128 (over z, y, core), tp: 4 (over x).
Axes of the slice: x: 4, y: 8, z: 8, core: 2. Of those that a mesh axis runs over, the one named last changes fastest.
Arguments:
- residual_in: bfloat16 [2560, 1024], P('ep', 'tp'), may hold values from -64 to 64
- queries: bfloat16 [2560, 512], P(('ep', 'tp')), may hold values from -6 to 6
- cache_keys: bfloat16 [2560, 1024, 128], P(('ep', 'tp')), may hold values from -6 to 6
- cache_values: bfloat16 [2560, 1024, 128], P(('ep', 'tp')), may hold values from -24 to 24
- lengths: int32 [2560], P(('ep', 'tp')), may hold values from 256 to 1024
- stick_offset: float32 [8], replicated, may hold values from 0.5 to 6
- out_weight: bfloat16 [512, 1024], P(None, 'tp'), may hold values from -0.25 to 0.25
- norm1_gain: float32 [1024], P('tp'), may hold values from 0.3 to 3.1
- norm1_bias: float32 [1024], P('tp'), may hold values from -1.5 to 1.5
- routes: int32 [2560, 6], P('ep'), may hold values from 0 to 127, all different within a row; in each aligned block of 20 rows (0 to 19, 20 to 39, ...) at most 2 rows name the same one
- route_weights: float32 [2560, 6], P('ep'), may hold values from 0.1 to 0.8
- expert_gate: bfloat16 [128, 1024, 512], P('ep', None, 'tp'), may hold values from -0.1875 to 0.1875
- expert_up: bfloat16 [128, 1024, 512], P('ep', None, 'tp'), may hold values from -0.1875 to 0.1875
- expert_down: bfloat16 [128, 512, 1024], P('ep', 'tp'), may hold values from -0.25 to 0.25
- shared_gate: bfloat16 [1024, 512], P(None, 'tp'), may hold values from -0.1875 to 0.1875
- shared_up: bfloat16 [1024, 512], P(None, 'tp'), may hold values from -0.1875 to 0.1875
- shared_down: bfloat16 [512, 1024], P('tp'), may hold values from -0.25 to 0.25
- norm2_gain: float32 [1024], P('tp'), may hold values from 0.1 to 1.9
- norm2_bias: float32 [1024], P('tp'), may hold values from -1.5 to 1.5
Outputs:
- layer_out: bfloat16 [2560, 1024], P('ep', 'tp')
Inputs may be any that keep to these rules, and one draw needn't show every extreme that they name: `routes`: each row names 6 different experts; among the rows of one index of ep no expert is named more than 2 times.
All inputs are finite; a program needn't handle non-finite values.
Results may differ from a plain program's by a relative error of at most 0.0095.
Values may be sent and summed in bfloat16 or wider, within the bound.
No kernel may reach another device: no remote copies, remote signals or barrier semaphores. Data moves between devices by JAX's collectives and lax.ppermute only.
A program may use at most 64 MiB of HBM per device.

v0:
```python
import jax
import jax.numpy as jnp
from jax import lax
from jax.sharding import PartitionSpec as P

H = 8
HD = 64
KVH = 2
CACHE = 1024
TOPK = 6


RESIDUAL_SCALE = 2.0**0.25
EPSILON = 1e-05


def joined_along(blocks, dim):
    blocks = jnp.moveaxis(blocks, 0, dim)
    shape = blocks.shape
    return blocks.reshape(*shape[:dim], shape[dim] * shape[dim + 1], *shape[dim + 2 :])


def from_everyone(value, axis):
    copies = jnp.broadcast_to(value, (lax.axis_size(axis), *value.shape))
    return lax.all_to_all(copies, axis, split_axis=0, concat_axis=0, tiled=True)


def gathered_copies(value, axis, dim):
    return joined_along(from_everyone(value, axis), dim)


def rows_first(arrays, axis, dims):
    turned = [jnp.moveaxis(a, dim, 0) for a, dim in zip(arrays, dims)]
    both = jnp.concatenate([t.reshape(len(t), -1) for t in turned], axis=1)
    out, at, done = (lax.all_gather(both, axis, axis=0, tiled=True), 0, [])
    for t, dim in zip(turned, dims):
        piece = out[:, at : at + t[0].size].reshape(-1, *t.shape[1:])
        done.append(jnp.moveaxis(piece, 0, dim))
        at += t[0].size
    return tuple(done)


def cut_along(value, dim, devices):
    before, after = (value.shape[:dim], value.shape[dim + 1 :])
    return jnp.moveaxis(value.reshape(*before, devices, -1, *after), dim, 0)


def sent_and_summed(value, axis, dim):
    blocks = cut_along(value, dim, lax.axis_size(axis))
    arrived = lax.all_to_all(blocks, axis, split_axis=0, concat_axis=0, tiled=True)
    return arrived.astype(jnp.float32).sum(axis=0)


def over_copies(value, axis):
    everything = from_everyone(value, axis)
    return jnp.sum(everything, axis=0)


def packed_total(arrays, axis):
    ends = [0]
    for a in arrays:
        ends.append(ends[-1] + a.size)
    running = over_copies(jnp.concatenate([a.ravel() for a in arrays]), axis)
    return tuple((running[b:e].reshape(a.shape) for a, b, e in zip(arrays, ends, ends[1:])))


def normalize(totals, squares, entries, values, scales, shifts):
    centre = totals / entries
    spread = squares / entries - centre * centre
    return (values - centre) * lax.rsqrt(spread + EPSILON) * scales + shifts


def stick_read(queries, keys_block, values_block, lengths, offsets):
    seq_count = queries.shape[0]
    grouped = H // KVH
    query_heads = queries.reshape(seq_count, KVH, grouped, HD)
    key_heads = keys_block.reshape(seq_count, CACHE, KVH, HD)
    value_heads = values_block.reshape(seq_count, CACHE, KVH, HD)
    scores = jnp.einsum(
        "sgjd,slgd->sgjl", query_heads, key_heads, preferred_element_type=jnp.float32
    )
    scores = scores * HD ** (-0.5) - offsets.reshape(1, KVH, grouped, 1)
    live_mask = (jnp.arange(CACHE)[None, :] < lengths[:, None])[:, None, None, :]
    keep_log = jnp.where(live_mask, jax.nn.log_sigmoid(-scores), 0.0)
    after_log = lax.cumsum(keep_log, axis=3, reverse=True) - keep_log
    weights = jnp.where(live_mask, jnp.exp(jax.nn.log_sigmoid(scores) + after_log), 0.0)
    weights = weights.astype(jnp.bfloat16)
    mixed = jnp.einsum("sgjl,slgd->sgjd", weights, value_heads, preferred_element_type=jnp.float32)
    return mixed.reshape(seq_count, H * HD).astype(jnp.bfloat16)


def body(
    residual_in,
    queries,
    cache_keys,
    cache_values,
    lengths,
    stick_offset,
    out_weight,
    norm1_gain,
    norm1_bias,
    routes,
    route_weights,
    expert_gate,
    expert_up,
    expert_down,
    shared_gate,
    shared_up,
    shared_down,
    norm2_gain,
    norm2_bias,
):
    mixed = stick_read(queries, cache_keys, cache_values, lengths, stick_offset)
    attended = jnp.dot(
        gathered_copies(mixed, "tp", 0), out_weight, preferred_element_type=jnp.float32
    )
    before = RESIDUAL_SCALE * residual_in.astype(jnp.float32) + attended
    group_rows, columns = residual_in.shape
    full_width = columns * lax.axis_size("tp")
    widened, scales, shifts = rows_first((before, norm1_gain, norm1_bias), "tp", (1, 0, 0))
    whole = normalize(
        jnp.sum(widened, axis=1, keepdims=True),
        jnp.sum(widened * widened, axis=1, keepdims=True),
        full_width,
        widened,
        scales,
        shifts,
    ).astype(jnp.bfloat16)
    normed = lax.dynamic_slice_in_dim(whole, lax.axis_index("tp") * columns, columns, 1)
    experts = lax.axis_size("ep")
    capacity = min(group_rows, 2 * ((group_rows * TOPK + experts - 1) // experts))
    slots_all = experts * capacity
    chosen = routes.reshape(-1)
    order_ids = jnp.arange(chosen.shape[0])
    matches = (chosen[:, None] == chosen[None, :]) & (order_ids[None, :] < order_ids[:, None])
    targets = chosen * capacity + jnp.sum(matches.astype(jnp.int32), axis=1)
    picks = (targets[:, None] == jnp.arange(slots_all)[None, :]).astype(jnp.float32)
    picks = picks.reshape(group_rows, TOPK, slots_all)
    dispatch = jnp.sum(picks, axis=1).astype(jnp.bfloat16)
    combine = jnp.sum(picks * route_weights[:, :, None], axis=1)
    parcel = jnp.einsum("sr,sd->rd", dispatch, whole, preferred_element_type=jnp.float32)
    parcel = parcel.astype(jnp.bfloat16).reshape(experts, capacity, full_width)
    arrived = lax.all_to_all(parcel, "ep", split_axis=0, concat_axis=0, tiled=True)
    gate_part = jnp.einsum(
        "ecd,df->ecf", arrived, expert_gate[0], preferred_element_type=jnp.float32
    )
    up_part = jnp.einsum("ecd,df->ecf", arrived, expert_up[0], preferred_element_type=jnp.float32)
    hidden = (jax.nn.silu(gate_part) * up_part).astype(jnp.bfloat16)
    partial_value = jnp.einsum(
        "ecf,fd->ecd", hidden, expert_down[0], preferred_element_type=jnp.float32
    )
    summed = sent_and_summed(partial_value.astype(jnp.bfloat16), "tp", 2).astype(jnp.bfloat16)
    returned = lax.all_to_all(summed, "ep", split_axis=0, concat_axis=0, tiled=True)
    routed = jnp.dot(
        combine,
        returned.reshape(slots_all, columns).astype(jnp.float32),
        precision=lax.Precision.HIGHEST,
    )
    shared_hidden = (
        jax.nn.silu(jnp.dot(whole, shared_gate, preferred_element_type=jnp.float32))
        * jnp.dot(whole, shared_up, preferred_element_type=jnp.float32)
    ).astype(jnp.bfloat16)
    shared_term = jnp.dot(shared_hidden, shared_down, preferred_element_type=jnp.float32)
    shared = sent_and_summed(shared_term.astype(jnp.bfloat16), "tp", 1)
    after = RESIDUAL_SCALE * normed.astype(jnp.float32) + routed + shared
    final_totals, final_squares = packed_total(
        (jnp.sum(after, axis=1), jnp.sum(after * after, axis=1)), "tp"
    )
    return normalize(
        final_totals[:, None], final_squares[:, None], full_width, after, norm2_gain, norm2_bias
    ).astype(jnp.bfloat16)


def solution(mesh):
    in_specs = (
        P("ep", "tp"),
        P(("ep", "tp"), None),
        P(("ep", "tp"), None, None),
        P(("ep", "tp"), None, None),
        P(("ep", "tp")),
        P(),
        P(None, "tp"),
        P("tp"),
        P("tp"),
        P("ep", None),
        P("ep", None),
        P("ep", None, "tp"),
        P("ep", None, "tp"),
        P("ep", "tp", None),
        P(None, "tp"),
        P(None, "tp"),
        P("tp", None),
        P("tp"),
        P("tp"),
    )
    out_specs = P("ep", "tp")
    return jax.shard_map(body, mesh=mesh, in_specs=in_specs, out_specs=out_specs, check_vma=False)
```

profile of v0, /device:TPU:1, one launch (start us, length us, event | category | flops | bytes accessed | tf_op | source)
XLA Modules:
  0.0 168.4 jit_solution(15376619532127802602)
XLA Ops:
  0.0 0.8 iota_compare_fusion.2
  0.8 1.6 copy.87
  2.4 0.1 reshape.116
  2.5 0.1 sub.42
  2.6 0.4 fusion.19
  3.1 49.5 %reduce-window.6 = f32[5,2,4,8,128]{4,3,2,1,0:T(8,128)S(1)} reduce-window(f32[5,2,4,8,128]{4,3,2,1,0:T(8,128)S(1)} %reshape.118, f32[]{:T(128)} %constant.30.clone.1), window={size=1x1x1x1x128 pad=0_0x0_0x0_0x0_0x0_127}, to_apply=%region_0.1 | reduce-window | flops 5201920 | bytes 327684 | tf_op jit(solution)/shard_map/reduce-window
  52.6 0.1 slice_reduce_fusion
  52.7 1.8 %reduce-window.9 = f32[5,2,4,9]{3,2,1,0:T(4,128)S(1)} reduce-window(f32[5,2,4,8]{3,2,1,0:T(4,128)S(1)} %slice_reduce_fusion, f32[]{:T(128)} %constant.30.clone.1), window={size=1x1x1x8 pad=0_0x0_0x0_0x0_8}, to_apply=%region_1.2 | reduce-window | flops 2520 | bytes 2724 | tf_op jit(solution)/shard_map/reduce-window.1
  54.5 0.1 slice.29
  54.6 0.1 broadcast_add_fusion
  54.8 0.6 copy.88
  55.5 0.6 convolution_convert_fusion.3
  56.1 0.1 convert_element_type.53
  56.2 0.6 broadcast_in_dim.19
  56.8 4.8 %all-to-all-start = ((bf16[4,5,512]{2,1,0:T(8,128)(2,1)}), bf16[4,5,512]{2,1,0:T(8,128)(2,1)S(1)}, u32[]{:S(2)}, u32[]{:S(2)}) async-start(bf16[4,5,512]{2,1,0:T(8,128)(2,1)} %broadcast_in_dim.19), calls=%async_computation | async-start | bytes 65536 | tf_op jit(solution)/shard_map/all_to_all | solution.py:25
  61.6 0.1 copy.89
  61.7 0.1 eq.29
  61.8 0.2 convert_reduce_fusion.2
  62.0 0.1 reduce_sum.98
  62.1 0.1 copy.90
  62.2 0.1 convert_reduce_fusion
  62.3 3.6 %all-to-all-done = bf16[4,5,512]{2,1,0:T(8,128)(2,1)S(1)} async-done(((bf16[4,5,512]{2,1,0:T(8,128)(2,1)}), bf16[4,5,512]{2,1,0:T(8,128)(2,1)S(1)}, u32[]{:S(2)}, u32[]{:S(2)}) %all-to-all-start) | async-done | bytes 20512 | tf_op jit(solution)/shard_map/all_to_all | solution.py:25
  66.0 0.2 fusion.3
  66.2 9.0 %all_gather.3 = f32[1024,22]{0,1:T(8,128)S(1)} all-gather(f32[256,22]{0,1:T(8,128)S(1)} %pad_maximum_fusion), channel_id=1, replica_groups=mesh['ep'=128,'tp'=4] {'tp'}, dimensions={0}, use_global_device_ids=true | all-gather | bytes 112640 | tf_op jit(solution)/shard_map/all_gather | solution.py:35
  75.2 0.1 slice_reduce_fusion.1
  75.4 0.1 add_convert_fusion
  75.5 0.3 convolution_convert_fusion.1
  75.8 0.2 reshape.124
  76.0 42.3 %all_to_all.31 = bf16[128,2,1024]{2,1,0:T(2,128)(2,1)S(1)} all-to-all(bf16[128,2,1024]{2,1,0:T(2,128)(2,1)S(1)} %reshape.124), channel_id=1, replica_groups=mesh['ep'=128,'tp'=4] {'ep'}, dimensions={0} | all-to-all | bytes 1048576 | tf_op jit(solution)/shard_map/all_to_all | solution.py:143
  118.3 0.3 fusion.7
  118.6 0.5 convolution_convert_fusion
  119.2 0.8 copy.107
  120.0 3.5 %all-to-all-start.2 = ((bf16[4,128,2,256]{3,1,2,0:T(8,128)(2,1)}), bf16[4,128,2,256]{3,1,2,0:T(8,128)(2,1)S(1)}, u32[]{:S(2)}, u32[]{:S(2)}) async-start(bf16[4,128,2,256]{3,1,2,0:T(8,128)(2,1)} %bitcast.48), calls=%async_computation.2 | async-start | bytes 1048576 | tf_op jit(solution)/shard_map/all_to_all | solution.py:50
  123.5 0.2 fusion.43
  123.7 0.3 convolution_convert_fusion.2
  124.0 0.6 copy.108
  124.6 8.6 %all-to-all-done.2 = bf16[4,128,2,256]{3,1,2,0:T(8,128)(2,1)S(1)} async-done(((bf16[4,128,2,256]{3,1,2,0:T(8,128)(2,1)}), bf16[4,128,2,256]{3,1,2,0:T(8,128)(2,1)S(1)}, u32[]{:S(2)}, u32[]{:S(2)}) %all-to-all-start.2) | async-done | bytes 524320 | tf_op jit(solution)/shard_map/all_to_all | solution.py:50
  133.3 3.3 %all-to-all-start.4 = ((bf16[4,20,256]{2,1,0:T(8,128)(2,1)}), bf16[4,20,256]{2,1,0:T(8,128)(2,1)S(1)}, u32[]{:S(2)}, u32[]{:S(2)}) async-start(bf16[4,20,256]{2,1,0:T(8,128)(2,1)} %bitcast.49), calls=%async_computation.4 | async-start | bytes 98304 | tf_op jit(solution)/shard_map/all_to_all | solution.py:50
  136.5 0.1 reduce_sum.101
  136.6 0.8 copy.95
  137.4 3.5 %all-to-all-done.4 = bf16[4,20,256]{2,1,0:T(8,128)(2,1)S(1)} async-done(((bf16[4,20,256]{2,1,0:T(8,128)(2,1)}), bf16[4,20,256]{2,1,0:T(8,128)(2,1)S(1)}, u32[]{:S(2)}, u32[]{:S(2)}) %all-to-all-start.4) | async-done | bytes 40992 | tf_op jit(solution)/shard_map/all_to_all | solution.py:50
  140.9 6.9 %all-to-all-start.3 = ((bf16[128,2,256]{2,1,0:T(2,128)(2,1)}), bf16[128,2,256]{2,1,0:T(2,128)(2,1)S(1)}, u32[]{:S(2)}, u32[]{:S(2)}) async-start(bf16[128,2,256]{2,1,0:T(2,128)(2,1)} %copy.95), calls=%async_computation.3 | async-start | bytes 262144 | tf_op jit(solution)/shard_map/all_to_all | solution.py:153
  147.9 12.8 %all-to-all-done.3 = bf16[128,2,256]{2,1,0:T(2,128)(2,1)S(1)} async-done(((bf16[128,2,256]{2,1,0:T(2,128)(2,1)}), bf16[128,2,256]{2,1,0:T(2,128)(2,1)S(1)}, u32[]{:S(2)}, u32[]{:S(2)}) %all-to-all-start.3) | async-done | bytes 131104 | tf_op jit(solution)/shard_map/all_to_all | solution.py:153
  160.7 0.3 fusion.41
  161.0 0.1 pad_maximum_fusion.1
  161.1 6.5 %all_to_all.32 = f32[4,1,40]{2,1,0:T(1,128)S(1)} all-to-all(f32[4,1,40]{2,1,0:T(1,128)S(1)} %broadcast_in_dim.20), channel_id=1, replica_groups=mesh['ep'=128,'tp'=4] {'tp'}, dimensions={0} | all-to-all | bytes 1280 | tf_op jit(solution)/shard_map/all_to_all | solution.py:25
  167.6 0.1 slice_multiply_fusion
  167.7 0.7 add_convert_fusion.1
  (46 shorter events, 0.4 us)
Async XLA Ops:
  0.0 118.6 %copy-start = (bf16[1,128,1024]{2,1,0:T(8,128)(2,1)S(1)}, bf16[1,128,1024]{2,1,0:T(8,128)(2,1)}, u32[]{:S(2)}) copy-start(bf16[1,128,1024]{2,1,0:T(8,128)(2,1)} %param.32) | copy-start | bytes 786436
  0.8 1.6 copy-start.8
  0.8 1.7 %copy-start.16 = (f32[8]{0:T(128)S(1)}, f32[8]{0:T(128)}, u32[]{:S(2)}) copy-start(f32[8]{0:T(128)} %param.24) | copy-start | bytes 100
  2.6 52.2 %copy-start.1 = (bf16[5,1024,128]{2,1,0:T(8,128)(2,1)S(1)}, bf16[5,1024,128]{2,1,0:T(8,128)(2,1)}, u32[]{:S(2)}) copy-start(bf16[5,1024,128]{2,1,0:T(8,128)(2,1)} %param.22) | copy-start | bytes 3932164
  55.4 6.2 %copy-start.6 = (s32[20,6]{0,1:T(8,128)S(1)}, s32[20,6]{0,1:T(8,128)}, u32[]{:S(2)}) copy-start(s32[20,6]{0,1:T(8,128)} %param.28) | copy-start | bytes 1444
  55.4 6.8 %copy-start.9 = (f32[20,6]{0,1:T(8,128)S(1)}, f32[20,6]{0,1:T(8,128)}, u32[]{:S(2)}) copy-start(f32[20,6]{0,1:T(8,128)} %param.29) | copy-start | bytes 1444
  55.4 10.5 %copy-start.2 = (bf16[512,256]{1,0:T(8,128)(2,1)S(1)}, bf16[512,256]{1,0:T(8,128)(2,1)}, u32[]{:S(2)}) copy-start(bf16[512,256]{1,0:T(8,128)(2,1)} %param.25) | copy-start | bytes 786436
  55.5 10.5 %copy-start.7 = (bf16[20,256]{1,0:T(8,128)(2,1)S(1)}, bf16[20,256]{1,0:T(8,128)(2,1)}, u32[]{:S(2)}) copy-start(bf16[20,256]{1,0:T(8,128)(2,1)} %param.19) | copy-start | bytes 30724
  55.5 10.7 %copy-start.10 = (f32[256]{0:T(256)S(1)}, f32[256]{0:T(256)}, u32[]{:S(2)}) copy-start(f32[256]{0:T(256)} %param.27) | copy-start | bytes 3076
  55.5 10.7 %copy-start.11 = (f32[256]{0:T(256)S(1)}, f32[256]{0:T(256)}, u32[]{:S(2)}) copy-start(f32[256]{0:T(256)} %param.26) | copy-start | bytes 3076
  56.8 9.1 %all-to-all-start = ((bf16[4,5,512]{2,1,0:T(8,128)(2,1)}), bf16[4,5,512]{2,1,0:T(8,128)(2,1)S(1)}, u32[]{:S(2)}, u32[]{:S(2)}) async-start(bf16[4,5,512]{2,1,0:T(8,128)(2,1)} %broadcast_in_dim.19), calls=%async_computation | async-start | bytes 65536 | tf_op jit(solution)/shard_map/all_to_all | solution.py:25
  75.5 42.8 %copy-start.14 = (bf16[1,1024,128]{2,1,0:T(8,128)(2,1)S(1)}, bf16[1,1024,128]{2,1,0:T(8,128)(2,1)}, u32[]{:S(2)}) copy-start(bf16[1,1024,128]{2,1,0:T(8,128)(2,1)} %param.30) | copy-start | bytes 786436
  75.8 42.8 %copy-start.15 = (bf16[1,1024,128]{2,1,0:T(8,128)(2,1)S(1)}, bf16[1,1024,128]{2,1,0:T(8,128)(2,1)}, u32[]{:S(2)}) copy-start(bf16[1,1024,128]{2,1,0:T(8,128)(2,1)} %param.31) | copy-start | bytes 786436
  119.1 4.3 %copy-start.3 = (bf16[1024,128]{1,0:T(8,128)(2,1)S(1)}, bf16[1024,128]{1,0:T(8,128)(2,1)}, u32[]{:S(2)}) copy-start(bf16[1024,128]{1,0:T(8,128)(2,1)} %param.33) | copy-start | bytes 786436
  119.1 4.5 %copy-start.4 = (bf16[128,1024]{1,0:T(8,128)(2,1)S(1)}, bf16[128,1024]{1,0:T(8,128)(2,1)}, u32[]{:S(2)}) copy-start(bf16[128,1024]{1,0:T(8,128)(2,1)} %param.35) | copy-start | bytes 786436
  119.2 4.5 %copy-start.5 = (bf16[1024,128]{1,0:T(8,128)(2,1)S(1)}, bf16[1024,128]{1,0:T(8,128)(2,1)}, u32[]{:S(2)}) copy-start(bf16[1024,128]{1,0:T(8,128)(2,1)} %param.34) | copy-start | bytes 786436
  120.0 13.3 %all-to-all-start.2 = ((bf16[4,128,2,256]{3,1,2,0:T(8,128)(2,1)}), bf16[4,128,2,256]{3,1,2,0:T(8,128)(2,1)S(1)}, u32[]{:S(2)}, u32[]{:S(2)}) async-start(bf16[4,128,2,256]{3,1,2,0:T(8,128)(2,1)} %bitcast.48), calls=%async_computation.2 | async-start | bytes 1048576 | tf_op jit(solution)/shard_map/all_to_all | solution.py:50
  123.7 44.0 %copy-start.12 = (f32[256]{0:T(256)S(1)}, f32[256]{0:T(256)}, u32[]{:S(2)}) copy-start(f32[256]{0:T(256)} %param.37) | copy-start | bytes 3076
  123.7 44.0 %copy-start.13 = (f32[256]{0:T(256)S(1)}, f32[256]{0:T(256)}, u32[]{:S(2)}) copy-start(f32[256]{0:T(256)} %param.36) | copy-start | bytes 3076
  133.3 7.6 %all-to-all-start.4 = ((bf16[4,20,256]{2,1,0:T(8,128)(2,1)}), bf16[4,20,256]{2,1,0:T(8,128)(2,1)S(1)}, u32[]{:S(2)}, u32[]{:S(2)}) async-start(bf16[4,20,256]{2,1,0:T(8,128)(2,1)} %bitcast.49), calls=%async_computation.4 | async-start | bytes 98304 | tf_op jit(solution)/shard_map/all_to_all | solution.py:50
  140.9 19.8 %all-to-all-start.3 = ((bf16[128,2,256]{2,1,0:T(2,128)(2,1)}), bf16[128,2,256]{2,1,0:T(2,128)(2,1)S(1)}, u32[]{:S(2)}, u32[]{:S(2)}) async-start(bf16[128,2,256]{2,1,0:T(2,128)(2,1)} %copy.95), calls=%async_computation.3 | async-start | bytes 262144 | tf_op jit(solution)/shard_map/all_to_all | solution.py:153
where the time goes:
time: 169 us; the launch traced here: 168 us
  blocking collectives  57.8 us (34%)
  other arithmetic  53.7 us (32%)
  waiting for transfers between devices  28.5 us (17%)
  starting transfers between devices  18.5 us (11%)
  local copies, waits for them, and re-layouts  6.46 us (4%)
  matrix products  3.03 us (2%)
    another operation x3, other arithmetic  51.4 us
    all_to_all x1, blocking collectives, body(): lax.all_to_all(parcel, 'ep', split_axis=0, concat_axis=0, tiled=True)  42.3 us
    all_to_all x1, waiting for transfers between devices, body(): lax.all_to_all(summed, 'ep', split_axis=0, concat_axis=0, tiled=True)  12.8 us
    all_to_all x2, waiting for transfers between devices, sent_and_summed(): lax.all_to_all(blocks, axis, split_axis=0, concat_axis=0, tiled=True)  12.1 us
    all_gather x1, blocking collectives, rows_first(): out, at, done = (lax.all_gather(both, axis, axis=0, tiled=True), 0, [])  9.04 us
    all_to_all x1, starting transfers between devices, body(): lax.all_to_all(summed, 'ep', split_axis=0, concat_axis=0, tiled=True)  6.93 us
    all_to_all x2, starting transfers between devices, sent_and_summed(): lax.all_to_all(blocks, axis, split_axis=0, concat_axis=0, tiled=True)  6.74 us
    all_to_all x1, blocking collectives, from_everyone(): return lax.all_to_all(copies, axis, split_axis=0, concat_axis=0, tiled=True)  6.47 us
  transfers between devices with their start and end apart: 4, of which 4 were waited for; matrix products, arithmetic and copies ran while one was open for 2% of the time, Pallas kernels for 0%

commit v1 on v0

v1 whole, which is shorter than its diff:
```python
import jax
import jax.numpy as jnp
from jax import lax
from jax.experimental import pallas as pl
from jax.experimental.pallas import tpu as pltpu
from jax.sharding import PartitionSpec as P

H = 8
HD = 64
KVH = 2
CACHE = 1024
TOPK = 6
LANES = 128
BLOCKS = CACHE // LANES

RESIDUAL_SCALE = 2.0**0.25
EPSILON = 1e-05


def stick_kernel(
    lengths, offsets, queries, keys, values, gate, up, down,
    out, packed, keys_vm, values_vm, reads, key_sems, value_sems, pack_sems,
):
    seqs = queries.shape[0]
    wide, hidden = gate.shape[1], gate.shape[2]
    key_copies = [
        pltpu.make_async_copy(keys.at[s], keys_vm.at[s], key_sems.at[s]) for s in range(seqs)
    ]
    value_copies = [
        pltpu.make_async_copy(values.at[s], values_vm.at[s], value_sems.at[s])
        for s in range(seqs)
    ]
    pieces = [(gate.at[0], 0, wide), (up.at[0], wide, wide)]
    for j in range(wide // LANES):
        piece = down.at[0, :, pl.ds(j * LANES, LANES)]
        pieces.append((piece, 2 * wide + j * hidden, hidden))
    pack_copies = [
        pltpu.make_async_copy(piece, packed.at[pl.ds(at, rows)], pack_sems.at[i])
        for i, (piece, at, rows) in enumerate(pieces)
    ]
    for copy in key_copies + value_copies + pack_copies:
        copy.start()

    row = lax.broadcasted_iota(jnp.int32, (H, LANES), 0)
    lane = lax.broadcasted_iota(jnp.int32, (H, LANES), 1)
    low = lane < HD
    first = row < H // KVH
    offset = jnp.zeros((H, LANES), jnp.float32)
    for h in range(H):
        offset = jnp.where(row == h, offsets[h], offset)
    wide_q = queries[...].astype(jnp.float32)
    place = lax.broadcasted_iota(jnp.int32, (LANES, 2 * LANES), 0)
    column = lax.broadcasted_iota(jnp.int32, (LANES, 2 * LANES), 1)
    later = jnp.where((place > column) | (column >= LANES), 1.0, 0.0).astype(jnp.bfloat16)

    stays, takes = [], []
    for s in range(seqs):
        query = jnp.zeros((H, LANES), jnp.float32)
        for h in range(H):
            pair = lax.slice(wide_q, (s, h // 2 * LANES), (s + 1, (h // 2 + 1) * LANES))
            both = jnp.broadcast_to(pair, (H, LANES))
            if h % 2 != h // (H // KVH):
                both = pltpu.roll(both, HD, 1)
            query = jnp.where(row == h, both, query)
        query = jnp.where(first == low, query, 0.0).astype(jnp.bfloat16)
        key_copies[s].wait()
        scores = lax.dot_general(
            query, keys_vm[s], (((1,), (1,)), ((), ())), preferred_element_type=jnp.float32
        )
        stay, take = [], []
        for b in range(BLOCKS):
            score = scores[:, b * LANES : (b + 1) * LANES] * HD ** (-0.5) - offset
            live = lane + b * LANES < lengths[s]
            tail = jnp.log1p(jnp.exp(-jnp.abs(score)))
            stay.append(jnp.where(live, jnp.minimum(-score, 0.0) - tail, 0.0))
            take.append(jnp.where(live, jnp.minimum(score, 0.0) - tail, -jnp.inf))
        stays.append(stay)
        takes.append(take)

    rest = jnp.concatenate([stays[s][b] for b in range(BLOCKS) for s in range(seqs)], axis=0)
    sums = jnp.zeros((BLOCKS * seqs * H, 2 * LANES), jnp.float32)
    for _ in range(3):
        part = rest.astype(jnp.bfloat16)
        sums = sums + jnp.dot(part, later, preferred_element_type=jnp.float32)
        rest = rest - part.astype(jnp.float32)

    weights = [[None] * BLOCKS for _ in range(seqs)]
    for s in range(seqs):
        beyond = jnp.zeros((H, LANES), jnp.float32)
        for b in reversed(range(BLOCKS)):
            at = (b * seqs + s) * H
            after = sums[at : at + H, :LANES] + beyond
            weights[s][b] = jnp.exp(takes[s][b] + after)
            beyond = beyond + sums[at : at + H, LANES:]

    for s in range(seqs):
        stick = jnp.concatenate(weights[s], axis=1).astype(jnp.bfloat16)
        value_copies[s].wait()
        mixed = jnp.dot(stick, values_vm[s], preferred_element_type=jnp.float32)
        mixed = jnp.where(low, mixed, pltpu.roll(mixed, H // KVH, 0))
        for h in range(H // KVH):
            reads[s : s + 1, h * LANES : (h + 1) * LANES] = mixed[h : h + 1, :]
    done = reads[0:seqs, :].astype(jnp.bfloat16)
    for d in range(out.shape[0]):
        out[d] = done
    for copy in pack_copies:
        copy.wait()


def stick_read(queries, keys, values, lengths, offsets, gate, up, down, copies):
    seqs = queries.shape[0]
    wide, hidden = gate.shape[1], gate.shape[2]
    anywhere = pl.BlockSpec(memory_space=pl.ANY)
    scalars = pl.BlockSpec(memory_space=pltpu.SMEM)
    vector = pl.BlockSpec(memory_space=pltpu.VMEM)
    return pl.pallas_call(
        stick_kernel,
        out_shape=(
            jax.ShapeDtypeStruct((copies, seqs, H * HD), jnp.bfloat16),
            jax.ShapeDtypeStruct((3 * wide, hidden), jnp.bfloat16),
        ),
        in_specs=[scalars, scalars, vector] + [anywhere] * 5,
        out_specs=(vector, anywhere),
        scratch_shapes=[
            pltpu.VMEM(keys.shape, jnp.bfloat16),
            pltpu.VMEM(values.shape, jnp.bfloat16),
            pltpu.VMEM((8, H * HD), jnp.float32),
            pltpu.SemaphoreType.DMA((seqs,)),
            pltpu.SemaphoreType.DMA((seqs,)),
            pltpu.SemaphoreType.DMA((2 + wide // LANES,)),
        ],
        name="stick",
    )(lengths, offsets, queries, keys, values, gate, up, down)


def expert_kernel(rows, gate, up, down, extra, out):
    wide, hidden = gate.shape[1], gate.shape[2]

    def half(gate_part, up_part):
        gated = jnp.dot(rows[...], gate_part, preferred_element_type=jnp.float32)
        upped = jnp.dot(rows[...], up_part, preferred_element_type=jnp.float32)
        return (gated / (1.0 + jnp.exp(-gated)) * upped).astype(jnp.bfloat16)

    own = half(gate[0], up[0])
    other = half(extra[0:wide], extra[wide : 2 * wide])
    for j in range(wide // LANES):
        at = 2 * wide + j * hidden
        piece = jnp.dot(
            own, down[0, :, j * LANES : (j + 1) * LANES], preferred_element_type=jnp.float32
        ) + jnp.dot(other, extra[at : at + hidden], preferred_element_type=jnp.float32)
        out[:, j * LANES : (j + 1) * LANES] = piece.astype(jnp.bfloat16)


def run_expert(rows, gate, up, down, extra):
    return pl.pallas_call(
        expert_kernel,
        out_shape=jax.ShapeDtypeStruct(rows.shape, jnp.bfloat16),
        in_specs=[pl.BlockSpec(memory_space=pltpu.VMEM)] * 5,
        out_specs=pl.BlockSpec(memory_space=pltpu.VMEM),
        name="expert",
    )(rows, gate, up, down, extra)


def exchanged(blocks, axis):
    return lax.all_to_all(blocks, axis, split_axis=0, concat_axis=0, tiled=True)


def moments(values, entries):
    centre = jnp.sum(values, axis=1, keepdims=True) / entries
    spread = jnp.sum(values * values, axis=1, keepdims=True) / entries - centre * centre
    return centre, lax.rsqrt(spread + EPSILON)


def body(
    residual_in,
    queries,
    cache_keys,
    cache_values,
    lengths,
    stick_offset,
    out_weight,
    norm1_gain,
    norm1_bias,
    routes,
    route_weights,
    expert_gate,
    expert_up,
    expert_down,
    shared_gate,
    shared_up,
    shared_down,
    norm2_gain,
    norm2_bias,
):
    peers = lax.axis_size("tp")
    experts = lax.axis_size("ep")
    place = lax.axis_index("tp")
    rows, columns = residual_in.shape
    wide = columns * peers
    mine = place % 2

    mixed, packed = stick_read(
        queries, cache_keys, cache_values, lengths, stick_offset,
        expert_gate, expert_up, expert_down, peers,
    )
    reads = exchanged(mixed, "tp").reshape(rows, H * HD)

    chosen = routes.reshape(-1)
    order = jnp.arange(chosen.shape[0])
    earlier = (chosen[:, None] == chosen[None, :]) & (order[None, :] < order[:, None])
    slots = jnp.sum(earlier.astype(jnp.int32), axis=1).reshape(routes.shape)
    target = jnp.where(slots == mine, routes, -1)
    picks = target[:, :, None] == jnp.arange(experts)[None, None, :]
    dispatch = jnp.sum(picks.astype(jnp.float32), axis=1).astype(jnp.bfloat16)
    combine = jnp.sum(jnp.where(picks, route_weights[:, :, None], 0.0), axis=1)

    weight = out_weight.reshape(KVH, H // KVH, HD, columns).swapaxes(0, 1)
    attended = jnp.dot(
        reads, weight.reshape(H * HD, columns), preferred_element_type=jnp.float32
    )
    before = RESIDUAL_SCALE * residual_in.astype(jnp.float32) + attended
    sent = jnp.concatenate([before, norm1_gain[None], norm1_bias[None]], axis=0)
    got = exchanged(jnp.broadcast_to(sent, (peers, *sent.shape)), "tp")
    got = got.swapaxes(0, 1).reshape(rows + 2, wide)
    widened = got[:rows]
    centre, scale = moments(widened, wide)
    whole = (widened - centre) * scale * got[rows] + got[rows + 1]
    whole = whole.astype(jnp.bfloat16)

    swaps = [(i, i ^ 1) for i in range(peers)]
    extra = lax.ppermute(packed, "tp", swaps)

    parcel = jnp.einsum("se,sd->ed", dispatch, whole, preferred_element_type=jnp.float32)
    parcel = parcel.astype(jnp.bfloat16).reshape(experts, wide // LANES, LANES)
    arrived = exchanged(parcel, "ep").reshape(experts, wide)
    produced = run_expert(arrived, expert_gate, expert_up, expert_down, extra)
    returned = exchanged(produced.reshape(experts, wide // LANES, LANES), "ep")
    routed = jnp.dot(
        combine,
        returned.reshape(experts, wide).astype(jnp.float32),
        precision=lax.Precision.HIGHEST,
    )
    shared_hidden = (
        jax.nn.silu(jnp.dot(whole, shared_gate, preferred_element_type=jnp.float32))
        * jnp.dot(whole, shared_up, preferred_element_type=jnp.float32)
    ).astype(jnp.bfloat16)
    shared = jnp.dot(shared_hidden, shared_down, preferred_element_type=jnp.float32)
    partial = (routed + shared).astype(jnp.bfloat16)
    partials = exchanged(jnp.broadcast_to(partial, (peers, *partial.shape)), "tp")
    after = RESIDUAL_SCALE * whole.astype(jnp.float32) + jnp.sum(
        partials.astype(jnp.float32), axis=0
    )
    centre, scale = moments(after, wide)
    own = lax.dynamic_slice_in_dim(after, place * columns, columns, 1)
    return ((own - centre) * scale * norm2_gain + norm2_bias).astype(jnp.bfloat16)


def solution(mesh):
    in_specs = (
        P("ep", "tp"),
        P(("ep", "tp"), None),
        P(("ep", "tp"), None, None),
        P(("ep", "tp"), None, None),
        P(("ep", "tp")),
        P(),
        P(None, "tp"),
        P("tp"),
        P("tp"),
        P("ep", None),
        P("ep", None),
        P("ep", None, "tp"),
        P("ep", None, "tp"),
        P("ep", "tp", None),
        P(None, "tp"),
        P(None, "tp"),
        P("tp", None),
        P("tp"),
        P("tp"),
    )
    out_specs = P("ep", "tp")
    return jax.shard_map(body, mesh=mesh, in_specs=in_specs, out_specs=out_specs, check_vma=False)
```

time: 169 us -> 129 us (0.76)
  other arithmetic: 53.7 us -> 1.72 us
  Pallas kernels: 0 us -> 29.4 us
  blocking collectives: 57.8 us -> 38.3 us
  waiting for transfers between devices: 28.5 us -> 31.3 us
  starting transfers between devices: 18.5 us -> 20.5 us
  matrix products: 3.03 us -> 1.07 us
    another operation x4 -> x0, other arithmetic: 51.5 us -> none
    pallas_call x0 -> x2, Pallas kernels: none -> 29.4 us  [the longest x1 26.5 us: stick_read(): pl.pallas_call(stick_kernel, out_shape=(jax.ShapeDtypeStruct((copies, seq...]
    all_to_all x2 -> x1, blocking collectives: 48.7 us -> 38.3 us  [exchanged(): return lax.all_to_all(blocks, axis, split_axis=0, concat_axis=0, tiled=True)]
    all_gather x1 -> x0, blocking collectives: 9.04 us -> none  [rows_first(): out, at, done = (lax.all_gather(both, axis, axis=0, tiled=True), 0, [])]
    ppermute x0 -> x1, starting transfers between devices: none -> 3.36 us  [body(): extra = lax.ppermute(packed, 'tp', swaps)]
    all_to_all x4, waiting for transfers between devices: 28.5 us -> 31.3 us  [exchanged(): return lax.all_to_all(blocks, axis, split_axis=0, concat_axis=0, tiled=True)]
    dot_general x7 -> x3, matrix products: 2.59 us -> 0.62 us  [the longest x1 0.25 us: body(): jnp.einsum('se,sd->ed', dispatch, whole, preferred_element_type=jnp.float32)]
    reshape x8 -> x1, local copies, waits for them, and re-layouts: 1.91 us -> 0.02 us  [body(): reads = exchanged(mixed, 'tp').reshape(rows, H * HD)]
  transfers between devices with their start and end apart: 4 -> 5, of which waited for: 4 -> 4; matrix products, arithmetic and copies ran while one was open for 2% -> 3% of each run, Pallas kernels for 0% -> 0%
where the time goes in v1:
time: 129 us; the launch traced here: 128 us
  blocking collectives  38.3 us (30%)
  waiting for transfers between devices  31.3 us (24%)
  Pallas kernels  29.4 us (23%)
  starting transfers between devices  20.5 us (16%)
  local copies, waits for them, and re-layouts  5.36 us (4%)
  other arithmetic  1.72 us (1%)
    all_to_all x1, blocking collectives, exchanged(): return lax.all_to_all(blocks, axis, split_axis=0, concat_axis=0, tiled=True)  38.3 us
    all_to_all x4, waiting for transfers between devices, exchanged(): return lax.all_to_all(blocks, axis, split_axis=0, concat_axis=0, tiled=True)  31.3 us
    pallas_call x1, Pallas kernels, stick_read(): pl.pallas_call(stick_kernel, out_shape=(jax.ShapeDtypeStruct((copies, seq...  26.5 us
    all_to_all x4, starting transfers between devices, exchanged(): return lax.all_to_all(blocks, axis, split_axis=0, concat_axis=0, tiled=True)  17.1 us
    unnamed x32, local copies, waits for them, and re-layouts  3.63 us
    ppermute x1, starting transfers between devices, body(): extra = lax.ppermute(packed, 'tp', swaps)  3.36 us
    pallas_call x1, Pallas kernels, run_expert(): pl.pallas_call(expert_kernel, out_shape=jax.ShapeDtypeStruct(rows.shape,...  2.88 us
  transfers between devices with their start and end apart: 5, of which 4 were waited for; matrix products, arithmetic and copies ran while one was open for 3% of the time, Pallas kernels for 0%

profile of v1, /device:TPU:1, one launch (start us, length us, event | category | flops | bytes accessed | tf_op | source)
XLA Modules:
  0.0 128.0 jit_solution(8430697572320862537)
XLA Ops:
  0.0 0.0 copy-start
  0.0 0.0 copy-start.5
  0.0 0.0 copy-start.8
  0.0 0.0 copy-start.9
  0.0 26.5 %stick.1 = (bf16[4,5,512]{2,1,0:T(8,128)(2,1)}, bf16[3072,128]{1,0:T(8,128)(2,1)}) custom-call(s32[5]{0:T(128)} %lengths.1, f32[8]{0:T(128)} %offsets.1, bf16[5,512]{1,0:T(8,128)(2,1)} %queries.1, bf16[5,1024,128]{2,1,0:T(8,128)(2,1)} %keys.1, bf16[5,1024,128]{2,1,0:T(8,128)(2,1)} %values.1, bf16[1,1024,128]{2,1,0:T(8,128)(2,1)} %gate.3, ...), custom_call_target="tpu_custom_call" | custom-call | tf_op jit(solution)/shard_map/stick/pallas_call | solution.py:116
  26.6 0.0 copy-start.7
  26.6 4.8 %all-to-all-start = ((bf16[4,5,512]{2,1,0:T(8,128)(2,1)}), bf16[4,5,512]{2,1,0:T(8,128)(2,1)S(1)}, u32[]{:S(2)}, u32[]{:S(2)}) async-start(bf16[4,5,512]{2,1,0:T(8,128)(2,1)} %get-tuple-element.7), calls=%async_computation | async-start | bytes 65536 | tf_op jit(solution)/shard_map/all_to_all | solution.py:165
  31.4 3.4 %collective-permute-start = (bf16[3072,128]{1,0:T(8,128)(2,1)}, bf16[3072,128]{1,0:T(8,128)(2,1)S(1)}, u32[]{:S(2)}, u32[]{:S(2)}) collective-permute-start(bf16[3072,128]{1,0:T(8,128)(2,1)} %get-tuple-element.8), channel_id=1, source_target_pairs={{0,1},{1,0},{2,3},{3,2},{4,5},{5,4},{6,7},{7,6},{8,9},{9,8},{10,11... | collective-permute-start | bytes 2359304 | tf_op jit(solution)/shard_map/ppermute | solution.py:231
  34.8 0.0 copy-done.6
  34.8 0.1 copy.46
  34.9 0.1 eq.39
  35.0 0.2 convert_reduce_fusion.2
  35.2 0.1 eq.45
  35.3 0.1 copy.48
  35.4 0.0 copy-done.3
  35.4 0.3 all-to-all-done
  35.7 0.0 copy-done.5
  35.8 0.2 convolution_add_fusion.1
  35.9 0.0 copy-done.8
  35.9 0.0 copy-done.9
  36.0 0.6 broadcast_in_dim.41
  36.6 3.4 %all-to-all-start.1 = ((f32[4,22,256]{2,1,0:T(8,128)}), f32[4,22,256]{2,1,0:T(8,128)S(1)}, u32[]{:S(2)}, u32[]{:S(2)}) async-start(f32[4,22,256]{2,1,0:T(8,128)} %broadcast_in_dim.41), calls=%async_computation.1 | async-start | bytes 196608 | tf_op jit(solution)/shard_map/all_to_all | solution.py:165
  40.0 0.0 copy-done.7
  40.0 0.1 convert_reduce_fusion.1
  40.1 10.5 %all-to-all-done.1 = f32[4,22,256]{2,1,0:T(8,128)S(1)} async-done(((f32[4,22,256]{2,1,0:T(8,128)}), f32[4,22,256]{2,1,0:T(8,128)S(1)}, u32[]{:S(2)}, u32[]{:S(2)}) %all-to-all-start.1) | async-done | bytes 90144 | tf_op jit(solution)/shard_map/all_to_all | solution.py:165
  50.7 0.2 slice_reduce_fusion
  50.9 0.1 add_convert_fusion.1
  51.1 0.1 add_convert_fusion
  51.2 0.3 fusion
  51.5 38.3 %all_to_all.25 = bf16[128,8,128]{2,1,0:T(8,128)(2,1)S(1)} all-to-all(bf16[128,8,128]{2,1,0:T(8,128)(2,1)S(1)} %bitcast.47), channel_id=1, replica_groups=mesh['ep'=128,'tp'=4] {'ep'}, dimensions={0} | all-to-all | bytes 524288 | tf_op jit(solution)/shard_map/all_to_all | solution.py:165
  89.8 0.8 copy.64
  90.5 0.0 collective-permute-done.extra
  90.5 0.9 copy-done.1
  91.4 2.9 %expert.1 = bf16[128,1024]{1,0:T(8,128)(2,1)} custom-call(bf16[128,1024]{1,0:T(8,128)(2,1)} %bitcast.49, bf16[1,1024,128]{2,1,0:T(8,128)(2,1)} %gate.3, bf16[1,1024,128]{2,1,0:T(8,128)(2,1)} %up.3, bf16[1,128,1024]{2,1,0:T(8,128)(2,1)} %down.3, bf16[3072,128]{1,0:T(8,128)(2,1)} %copy-done.1), custom_call_target="tpu_custom_call" | custom-call | tf_op jit(solution)/shard_map/expert/pallas_call | solution.py:155
  94.3 1.7 %copy.56 = bf16[16,8,8,128]{3,2,1,0:T(8,128)(2,1)} copy(bf16[16,8,8,128]{3,1,2,0:T(8,128)(2,1)} %bitcast.50) | data formatting | bytes 524288
  96.1 5.5 %all-to-all-start.3 = ((bf16[128,8,128]{2,1,0:T(8,128)(2,1)}), bf16[128,8,128]{2,1,0:T(8,128)(2,1)S(1)}, u32[]{:S(2)}, u32[]{:S(2)}) async-start(bf16[128,8,128]{2,1,0:T(8,128)(2,1)} %bitcast.21), calls=%async_computation.3 | async-start | bytes 524288 | tf_op jit(solution)/shard_map/all_to_all | solution.py:165
  101.6 0.0 copy-done.2
  101.6 0.0 copy-start.10
  101.6 0.0 copy-start.11
  101.6 0.2 fusion.21
  101.8 15.2 %all-to-all-done.3 = bf16[128,8,128]{2,1,0:T(8,128)(2,1)S(1)} async-done(((bf16[128,8,128]{2,1,0:T(8,128)(2,1)}), bf16[128,8,128]{2,1,0:T(8,128)(2,1)S(1)}, u32[]{:S(2)}, u32[]{:S(2)}) %all-to-all-start.3) | async-done | bytes 262176 | tf_op jit(solution)/shard_map/all_to_all | solution.py:165
  117.0 0.2 fusion.3
  117.2 0.3 fusion.1
  117.5 0.7 broadcast_in_dim.45
  118.2 3.4 %all-to-all-start.4 = ((bf16[4,20,1024]{2,1,0:T(8,128)(2,1)}), bf16[4,20,1024]{2,1,0:T(8,128)(2,1)S(1)}, u32[]{:S(2)}, u32[]{:S(2)}) async-start(bf16[4,20,1024]{2,1,0:T(8,128)(2,1)} %broadcast_in_dim.45), calls=%async_computation.4 | async-start | bytes 393216 | tf_op jit(solution)/shard_map/all_to_all | solution.py:165
  121.6 5.4 %all-to-all-done.4 = bf16[4,20,1024]{2,1,0:T(8,128)(2,1)S(1)} async-done(((bf16[4,20,1024]{2,1,0:T(8,128)(2,1)}), bf16[4,20,1024]{2,1,0:T(8,128)(2,1)S(1)}, u32[]{:S(2)}, u32[]{:S(2)}) %all-to-all-start.4) | async-done | bytes 163872 | tf_op jit(solution)/shard_map/all_to_all | solution.py:165
  127.0 0.2 fusion.7
  127.3 0.7 fusion.12
  (25 shorter events, 0.3 us)
Async XLA Ops:
  0.0 117.2 %copy-start = (bf16[128,1024]{1,0:T(8,128)(2,1)S(1)}, bf16[128,1024]{1,0:T(8,128)(2,1)}, u32[]{:S(2)}) copy-start(bf16[128,1024]{1,0:T(8,128)(2,1)} %param.35) | copy-start | bytes 786436
  0.0 34.8 %copy-start.6 = (s32[20,6]{0,1:T(8,128)S(1)}, s32[20,6]{0,1:T(8,128)}, u32[]{:S(2)}) copy-start(s32[20,6]{0,1:T(8,128)} %param.28) | copy-start | bytes 1444
  0.0 35.4 %copy-start.3 = (bf16[512,256]{1,0:T(8,128)(2,1)S(1)}, bf16[512,256]{1,0:T(8,128)(2,1)}, u32[]{:S(2)}) copy-start(bf16[512,256]{1,0:T(8,128)(2,1)} %param.25) | copy-start | bytes 786436
  0.0 35.7 %copy-start.5 = (bf16[20,256]{1,0:T(8,128)(2,1)S(1)}, bf16[20,256]{1,0:T(8,128)(2,1)}, u32[]{:S(2)}) copy-start(bf16[20,256]{1,0:T(8,128)(2,1)} %param.19) | copy-start | bytes 30724
  0.0 35.9 %copy-start.8 = (f32[256]{0:T(256)S(1)}, f32[256]{0:T(256)}, u32[]{:S(2)}) copy-start(f32[256]{0:T(256)} %param.27) | copy-start | bytes 3076
  0.0 35.9 %copy-start.9 = (f32[256]{0:T(256)S(1)}, f32[256]{0:T(256)}, u32[]{:S(2)}) copy-start(f32[256]{0:T(256)} %param.26) | copy-start | bytes 3076
  26.6 13.4 %copy-start.7 = (f32[20,6]{0,1:T(8,128)S(1)}, f32[20,6]{0,1:T(8,128)}, u32[]{:S(2)}) copy-start(f32[20,6]{0,1:T(8,128)} %param.29) | copy-start | bytes 1444
  26.6 9.1 %all-to-all-start = ((bf16[4,5,512]{2,1,0:T(8,128)(2,1)}), bf16[4,5,512]{2,1,0:T(8,128)(2,1)S(1)}, u32[]{:S(2)}, u32[]{:S(2)}) async-start(bf16[4,5,512]{2,1,0:T(8,128)(2,1)} %get-tuple-element.7), calls=%async_computation | async-start | bytes 65536 | tf_op jit(solution)/shard_map/all_to_all | solution.py:165
  31.4 59.1 %collective-permute-start = (bf16[3072,128]{1,0:T(8,128)(2,1)}, bf16[3072,128]{1,0:T(8,128)(2,1)S(1)}, u32[]{:S(2)}, u32[]{:S(2)}) collective-permute-start(bf16[3072,128]{1,0:T(8,128)(2,1)} %get-tuple-element.8), channel_id=1, source_target_pairs={{0,1},{1,0},{2,3},{3,2},{4,5},{5,4},{6,7},{7,6},{8,9},{9,8},{10,11... | collective-permute-start | bytes 2359304 | tf_op jit(solution)/shard_map/ppermute | solution.py:231
  36.6 14.0 %all-to-all-start.1 = ((f32[4,22,256]{2,1,0:T(8,128)}), f32[4,22,256]{2,1,0:T(8,128)S(1)}, u32[]{:S(2)}, u32[]{:S(2)}) async-start(f32[4,22,256]{2,1,0:T(8,128)} %broadcast_in_dim.41), calls=%async_computation.1 | async-start | bytes 196608 | tf_op jit(solution)/shard_map/all_to_all | solution.py:165
  90.5 0.9 copy-start.1
  91.4 10.2 %copy-start.2 = (bf16[1024,128]{1,0:T(8,128)(2,1)S(1)}, bf16[1024,128]{1,0:T(8,128)(2,1)}, u32[]{:S(2)}) copy-start(bf16[1024,128]{1,0:T(8,128)(2,1)} %param.33) | copy-start | bytes 786436
  94.3 22.9 %copy-start.4 = (bf16[1024,128]{1,0:T(8,128)(2,1)S(1)}, bf16[1024,128]{1,0:T(8,128)(2,1)}, u32[]{:S(2)}) copy-start(bf16[1024,128]{1,0:T(8,128)(2,1)} %param.34) | copy-start | bytes 786436
  96.1 20.9 %all-to-all-start.3 = ((bf16[128,8,128]{2,1,0:T(8,128)(2,1)}), bf16[128,8,128]{2,1,0:T(8,128)(2,1)S(1)}, u32[]{:S(2)}, u32[]{:S(2)}) async-start(bf16[128,8,128]{2,1,0:T(8,128)(2,1)} %bitcast.21), calls=%async_computation.3 | async-start | bytes 524288 | tf_op jit(solution)/shard_map/all_to_all | solution.py:165
  101.6 25.6 %copy-start.10 = (f32[256]{0:T(256)S(1)}, f32[256]{0:T(256)}, u32[]{:S(2)}) copy-start(f32[256]{0:T(256)} %param.37) | copy-start | bytes 3076
  101.6 25.6 %copy-start.11 = (f32[256]{0:T(256)S(1)}, f32[256]{0:T(256)}, u32[]{:S(2)}) copy-start(f32[256]{0:T(256)} %param.36) | copy-start | bytes 3076
  118.2 8.7 %all-to-all-start.4 = ((bf16[4,20,1024]{2,1,0:T(8,128)(2,1)}), bf16[4,20,1024]{2,1,0:T(8,128)(2,1)S(1)}, u32[]{:S(2)}, u32[]{:S(2)}) async-start(bf16[4,20,1024]{2,1,0:T(8,128)(2,1)} %broadcast_in_dim.45), calls=%async_computation.4 | async-start | bytes 393216 | tf_op jit(solution)/shard_map/all_to_all | solution.py:165

commit v2 on v1

--- a/solution.py
+++ b/solution.py
@@ -1,3 +1,5 @@
+import functools
+
 import jax
 import jax.numpy as jnp
 from jax import lax
@@ -12,6 +14,9 @@
 TOPK = 6
 LANES = 128
 BLOCKS = CACHE // LANES
+PADDED = 8
+GROUP = 24
+GRANT = pltpu.CompilerParams(vmem_limit_bytes=12 << 20)
 
 RESIDUAL_SCALE = 2.0**0.25
 EPSILON = 1e-05
@@ -100,7 +105,8 @@
         mixed = jnp.where(low, mixed, pltpu.roll(mixed, H // KVH, 0))
         for h in range(H // KVH):
             reads[s : s + 1, h * LANES : (h + 1) * LANES] = mixed[h : h + 1, :]
-    done = reads[0:seqs, :].astype(jnp.bfloat16)
+    reads[seqs:, :] = jnp.zeros((reads.shape[0] - seqs, H * HD), jnp.float32)
+    done = reads[...].astype(jnp.bfloat16)
     for d in range(out.shape[0]):
         out[d] = done
     for copy in pack_copies:
@@ -110,65 +116,240 @@
 def stick_read(queries, keys, values, lengths, offsets, gate, up, down, copies):
     seqs = queries.shape[0]
     wide, hidden = gate.shape[1], gate.shape[2]
-    anywhere = pl.BlockSpec(memory_space=pl.ANY)
+    anywhere = pl.BlockSpec(memory_space=pltpu.HBM)
     scalars = pl.BlockSpec(memory_space=pltpu.SMEM)
     vector = pl.BlockSpec(memory_space=pltpu.VMEM)
     return pl.pallas_call(
         stick_kernel,
         out_shape=(
-            jax.ShapeDtypeStruct((copies, seqs, H * HD), jnp.bfloat16),
+            jax.ShapeDtypeStruct((copies, PADDED, H * HD), jnp.bfloat16),
             jax.ShapeDtypeStruct((3 * wide, hidden), jnp.bfloat16),
         ),
         in_specs=[scalars, scalars, vector] + [anywhere] * 5,
-        out_specs=(vector, anywhere),
+        out_specs=(vector, vector),
         scratch_shapes=[
             pltpu.VMEM(keys.shape, jnp.bfloat16),
             pltpu.VMEM(values.shape, jnp.bfloat16),
-            pltpu.VMEM((8, H * HD), jnp.float32),
+            pltpu.VMEM((PADDED, H * HD), jnp.float32),
             pltpu.SemaphoreType.DMA((seqs,)),
             pltpu.SemaphoreType.DMA((seqs,)),
             pltpu.SemaphoreType.DMA((2 + wide // LANES,)),
         ],
+        compiler_params=GRANT,
         name="stick",
-    )(lengths, offsets, queries, keys, values, gate, up, down)
-
-
-def expert_kernel(rows, gate, up, down, extra, out):
-    wide, hidden = gate.shape[1], gate.shape[2]
-
-    def half(gate_part, up_part):
-        gated = jnp.dot(rows[...], gate_part, preferred_element_type=jnp.float32)
-        upped = jnp.dot(rows[...], up_part, preferred_element_type=jnp.float32)
+    )(*(
+        pltpu.with_memory_space_constraint(x, pltpu.HBM)
+        for x in (lengths, offsets, queries, keys, values, gate, up, down)
+    ))
+
+
+def project_kernel(reads, weight, residual, gain, bias, out):
+    sources, seqs = out.shape[0], residual.shape[0] // out.shape[0]
+    rows, columns = residual.shape
+    token = lax.broadcasted_iota(jnp.int32, (GROUP, reads.shape[0]), 0)
+    arrived = lax.broadcasted_iota(jnp.int32, (GROUP, reads.shape[0]), 1)
+    held = jnp.zeros((GROUP, reads.shape[0]), jnp.bool_)
+    for t in range(sources):
+        inside = (token >= t * seqs) & (token < (t + 1) * seqs)
+        held = held | (inside & (arrived == token + t * (PADDED - seqs)))
+    held = jnp.where(held, 1.0, 0.0).astype(jnp.bfloat16)
+    mixed = jnp.dot(held, reads[...], preferred_element_type=jnp.float32).astype(jnp.bfloat16)
+    pairs = H // KVH
+    attended = jnp.zeros((GROUP, columns), jnp.float32)
+    for h in range(pairs):
+        part = jnp.concatenate(
+            [weight[h * HD : (h + 1) * HD], weight[(pairs + h) * HD : (pairs + h + 1) * HD]], axis=0
+        )
+        attended = attended + jnp.dot(
+            mixed[:, h * LANES : (h + 1) * LANES], part, preferred_element_type=jnp.float32
+        )
+    before = RESIDUAL_SCALE * residual[...].astype(jnp.float32) + attended[0:rows]
+    rest = jnp.zeros((GROUP - rows - 2, columns), jnp.float32)
+    for d in range(sources):
+        out[d, 0:rows] = before
+        out[d, rows : rows + 1] = gain[...]
+        out[d, rows + 1 : rows + 2] = bias[...]
+        out[d, rows + 2 :] = rest
+
+
+def project(reads, weight, residual, gain, bias, copies):
+    columns = weight.shape[1]
+    vector = pl.BlockSpec(memory_space=pltpu.VMEM)
+    return pl.pallas_call(
+        project_kernel,
+        out_shape=jax.ShapeDtypeStruct((copies, GROUP, columns), jnp.float32),
+        in_specs=[vector] * 5,
+        out_specs=vector,
+        compiler_params=GRANT,
+        name="project",
+    )(reads, weight, residual, gain.reshape(1, -1), bias.reshape(1, -1))
+
+
+def row_moments(blocks, entries):
+    total = blocks[0]
+    squares = blocks[0] * blocks[0]
+    for block in blocks[1:]:
+        total = total + block
+        squares = squares + block * block
+    centre = jnp.sum(total, axis=1, keepdims=True) / entries
+    spread = jnp.sum(squares, axis=1, keepdims=True) / entries - centre * centre
+    return centre, lax.rsqrt(spread + EPSILON)
+
+
+def norm_kernel(rows, got, dispatch, whole, parcel):
+    blocks = []
+    for t in range(got.shape[0]):
+        for j in range(got.shape[2] // LANES):
+            blocks.append(got[t, :, j * LANES : (j + 1) * LANES])
+    centre, scale = row_moments(blocks, len(blocks) * LANES)
+    normed = []
+    for j, block in enumerate(blocks):
+        value = (block - centre) * scale * block[rows : rows + 1] + block[rows + 1 : rows + 2]
+        normed.append(value)
+        whole[:, j * LANES : (j + 1) * LANES] = value.astype(jnp.bfloat16)
+    stacked = jnp.concatenate(normed, axis=0).astype(jnp.bfloat16)
+    parcel[...] = jnp.dot(
+        dispatch[...], stacked, preferred_element_type=jnp.float32
+    ).astype(jnp.bfloat16)
+
+
+def normalize_and_pick(got, dispatch, rows):
+    wide = got.shape[0] * got.shape[2]
+    vector = pl.BlockSpec(memory_space=pltpu.VMEM)
+    return pl.pallas_call(
+        functools.partial(norm_kernel, rows),
+        out_shape=(
+            jax.ShapeDtypeStruct((GROUP, wide), jnp.bfloat16),
+            jax.ShapeDtypeStruct((dispatch.shape[0], LANES), jnp.bfloat16),
+        ),
+        in_specs=[vector] * 2,
+        out_specs=(vector, vector),
+        compiler_params=GRANT,
+        name="norm",
+    )(got, dispatch)
+
+
+def expert_kernel(rows, packed, side, out, turned):
+    count, blocks = turned.shape[0], turned.shape[1]
+    wide, hidden = blocks * LANES, packed.shape[1]
+    turned[...] = rows[...].astype(jnp.float32).reshape(turned.shape)
+    features = jnp.concatenate(
+        [turned[:, j, :].astype(jnp.bfloat16) for j in range(blocks)], axis=1
+    )
+
+    def silu_times(weights):
+        gated = jnp.dot(features, weights[0:wide], preferred_element_type=jnp.float32)
+        upped = jnp.dot(features, weights[wide : 2 * wide], preferred_element_type=jnp.float32)
         return (gated / (1.0 + jnp.exp(-gated)) * upped).astype(jnp.bfloat16)
 
-    own = half(gate[0], up[0])
-    other = half(extra[0:wide], extra[wide : 2 * wide])
-    for j in range(wide // LANES):
+    own = silu_times(packed)
+    other = silu_times(side)
+    for j in range(blocks):
         at = 2 * wide + j * hidden
-        piece = jnp.dot(
-            own, down[0, :, j * LANES : (j + 1) * LANES], preferred_element_type=jnp.float32
-        ) + jnp.dot(other, extra[at : at + hidden], preferred_element_type=jnp.float32)
-        out[:, j * LANES : (j + 1) * LANES] = piece.astype(jnp.bfloat16)
-
-
-def run_expert(rows, gate, up, down, extra):
+        turned[:, j, :] = jnp.dot(
+            own, packed[at : at + hidden], preferred_element_type=jnp.float32
+        ) + jnp.dot(other, side[at : at + hidden], preferred_element_type=jnp.float32)
+    out[...] = turned[...].reshape(out.shape).astype(jnp.bfloat16)
+
+
+def run_expert(rows, packed, side, count):
+    blocks = rows.shape[0] // count
+    vector = pl.BlockSpec(memory_space=pltpu.VMEM)
     return pl.pallas_call(
         expert_kernel,
         out_shape=jax.ShapeDtypeStruct(rows.shape, jnp.bfloat16),
-        in_specs=[pl.BlockSpec(memory_space=pltpu.VMEM)] * 5,
-        out_specs=pl.BlockSpec(memory_space=pltpu.VMEM),
+        in_specs=[vector] * 3,
+        out_specs=vector,
+        scratch_shapes=[pltpu.VMEM((count, blocks, LANES), jnp.float32)],
+        compiler_params=GRANT,
         name="expert",
-    )(rows, gate, up, down, extra)
+    )(rows, packed, side)
+
+
+def combine_kernel(high, low, returned, shared, out):
+    total = high.shape[0]
+    sums = jnp.dot(high[...], returned[...], preferred_element_type=jnp.float32)
+    sums = sums + jnp.dot(low[...], returned[...], preferred_element_type=jnp.float32)
+    for j in range(total // GROUP):
+        at = slice(j * LANES, (j + 1) * LANES)
+        piece = (sums[j * GROUP : (j + 1) * GROUP] + shared[:, at]).astype(jnp.bfloat16)
+        for d in range(out.shape[0]):
+            out[d, :, at] = piece
+
+
+def combine_parts(combine, returned, shared, copies):
+    vector = pl.BlockSpec(memory_space=pltpu.VMEM)
+    return pl.pallas_call(
+        combine_kernel,
+        out_shape=jax.ShapeDtypeStruct((copies, *shared.shape), jnp.bfloat16),
+        in_specs=[vector] * 4,
+        out_specs=vector,
+        compiler_params=GRANT,
+        name="combine",
+    )(*combine, returned, shared)
+
+
+def finish_kernel(place, partials, whole, gain, bias, out, after):
+    rows, columns = out.shape
+    blocks = []
+    for j in range(whole.shape[1] // LANES):
+        at = slice(j * LANES, (j + 1) * LANES)
+        block = RESIDUAL_SCALE * whole[:, at].astype(jnp.float32)
+        for d in range(partials.shape[0]):
+            block = block + partials[d, :, at].astype(jnp.float32)
+        after[:, at] = block
+        blocks.append(block)
+    centre, scale = row_moments(blocks, len(blocks) * LANES)
+    start = pl.multiple_of(place[0] * columns, columns)
+    own = after[:, pl.ds(start, columns)]
+    own = (own - centre) * scale * gain[...] + bias[...]
+    out[...] = own[0:rows].astype(jnp.bfloat16)
+
+
+def finish(place, partials, whole, gain, bias, rows):
+    vector = pl.BlockSpec(memory_space=pltpu.VMEM)
+    return pl.pallas_call(
+        finish_kernel,
+        out_shape=jax.ShapeDtypeStruct((rows, gain.shape[0]), jnp.bfloat16),
+        in_specs=[pl.BlockSpec(memory_space=pltpu.SMEM)] + [vector] * 4,
+        out_specs=vector,
+        scratch_shapes=[pltpu.VMEM(whole.shape, jnp.float32)],
+        compiler_params=GRANT,
+        name="finish",
+    )(place.reshape(1), partials, whole, gain.reshape(1, -1), bias.reshape(1, -1))
 
 
 def exchanged(blocks, axis):
     return lax.all_to_all(blocks, axis, split_axis=0, concat_axis=0, tiled=True)
 
 
-def moments(values, entries):
-    centre = jnp.sum(values, axis=1, keepdims=True) / entries
-    spread = jnp.sum(values * values, axis=1, keepdims=True) / entries - centre * centre
-    return centre, lax.rsqrt(spread + EPSILON)
+def padded_rows(values, fill):
+    short = GROUP - values.shape[0]
+    return jnp.pad(values, ((0, short), (0, 0)), constant_values=fill)
+
+
+def picks_of(routes, route_weights, mine, experts, blocks):
+    chosen = routes.reshape(-1)
+    order = jnp.arange(chosen.shape[0])
+    earlier = (chosen[:, None] == chosen[None, :]) & (order[None, :] < order[:, None])
+    slots = jnp.sum(earlier.astype(jnp.int32), axis=1).reshape(routes.shape)
+    target = padded_rows(jnp.where(slots == mine, routes, -1), -1)
+    weight = padded_rows(route_weights, 0.0)
+    target = jnp.tile(target, (blocks, 1))
+    weight = jnp.tile(weight, (blocks, 1))
+    shape = (blocks * GROUP, experts * blocks)
+    block = lax.broadcasted_iota(jnp.int32, shape, 0) // GROUP
+    column = lax.broadcasted_iota(jnp.int32, shape, 1)
+    expert = jnp.where(column % blocks == block, column // blocks, -2)
+    picked = jnp.zeros(shape, jnp.float32)
+    combine = jnp.zeros(shape, jnp.float32)
+    for k in range(routes.shape[1]):
+        hit = target[:, k : k + 1] == expert
+        picked = picked + jnp.where(hit, 1.0, 0.0)
+        combine = combine + jnp.where(hit, weight[:, k : k + 1], 0.0)
+    high = lax.reduce_precision(combine, 8, 7)
+    parts = (high.astype(jnp.bfloat16), (combine - high).astype(jnp.bfloat16))
+    return picked.T.astype(jnp.bfloat16), parts
 
 
 def body(
@@ -197,62 +378,38 @@
     place = lax.axis_index("tp")
     rows, columns = residual_in.shape
     wide = columns * peers
-    mine = place % 2
+    blocks = wide // LANES
 
     mixed, packed = stick_read(
         queries, cache_keys, cache_values, lengths, stick_offset,
         expert_gate, expert_up, expert_down, peers,
     )
-    reads = exchanged(mixed, "tp").reshape(rows, H * HD)
-
-    chosen = routes.reshape(-1)
-    order = jnp.arange(chosen.shape[0])
-    earlier = (chosen[:, None] == chosen[None, :]) & (order[None, :] < order[:, None])
-    slots = jnp.sum(earlier.astype(jnp.int32), axis=1).reshape(routes.shape)
-    target = jnp.where(slots == mine, routes, -1)
-    picks = target[:, :, None] == jnp.arange(experts)[None, None, :]
-    dispatch = jnp.sum(picks.astype(jnp.float32), axis=1).astype(jnp.bfloat16)
-    combine = jnp.sum(jnp.where(picks, route_weights[:, :, None], 0.0), axis=1)
-
-    weight = out_weight.reshape(KVH, H // KVH, HD, columns).swapaxes(0, 1)
-    attended = jnp.dot(
-        reads, weight.reshape(H * HD, columns), preferred_element_type=jnp.float32
-    )
-    before = RESIDUAL_SCALE * residual_in.astype(jnp.float32) + attended
-    sent = jnp.concatenate([before, norm1_gain[None], norm1_bias[None]], axis=0)
-    got = exchanged(jnp.broadcast_to(sent, (peers, *sent.shape)), "tp")
-    got = got.swapaxes(0, 1).reshape(rows + 2, wide)
-    widened = got[:rows]
-    centre, scale = moments(widened, wide)
-    whole = (widened - centre) * scale * got[rows] + got[rows + 1]
-    whole = whole.astype(jnp.bfloat16)
-
-    swaps = [(i, i ^ 1) for i in range(peers)]
-    extra = lax.ppermute(packed, "tp", swaps)
-
-    parcel = jnp.einsum("se,sd->ed", dispatch, whole, preferred_element_type=jnp.float32)
-    parcel = parcel.astype(jnp.bfloat16).reshape(experts, wide // LANES, LANES)
-    arrived = exchanged(parcel, "ep").reshape(experts, wide)
-    produced = run_expert(arrived, expert_gate, expert_up, expert_down, extra)
-    returned = exchanged(produced.reshape(experts, wide // LANES, LANES), "ep")
-    routed = jnp.dot(
-        combine,
-        returned.reshape(experts, wide).astype(jnp.float32),
-        precision=lax.Precision.HIGHEST,
-    )
+    reads = exchanged(mixed, "tp").reshape(peers * PADDED, H * HD)
+    dispatch, combine = picks_of(routes, route_weights, place % 2, experts, blocks)
+    sent = project(reads, out_weight, residual_in, norm1_gain, norm1_bias, peers)
+    got = exchanged(sent, "tp")
+
+    swaps = []
+    for e in range(experts):
+        for t in range(peers):
+            partner = t ^ 1 if e % 2 == 0 else ((t + 1) ^ 1) - 1
+            swaps.append((e * peers + t, e * peers + partner % peers))
+    side = lax.ppermute(packed, ("ep", "tp"), swaps)
+
+    whole, parcel = normalize_and_pick(got, dispatch, rows)
+    arrived = exchanged(parcel.reshape(experts, blocks, LANES), "ep")
+    produced = run_expert(arrived.reshape(experts * blocks, LANES), packed, side, experts)
+    returned = exchanged(produced.reshape(experts, blocks, LANES), "ep")
     shared_hidden = (
         jax.nn.silu(jnp.dot(whole, shared_gate, preferred_element_type=jnp.float32))
         * jnp.dot(whole, shared_up, preferred_element_type=jnp.float32)
     ).astype(jnp.bfloat16)
     shared = jnp.dot(shared_hidden, shared_down, preferred_element_type=jnp.float32)
-    partial = (routed + shared).astype(jnp.bfloat16)
-    partials = exchanged(jnp.broadcast_to(partial, (peers, *partial.shape)), "tp")
-    after = RESIDUAL_SCALE * whole.astype(jnp.float32) + jnp.sum(
-        partials.astype(jnp.float32), axis=0
+    partial = combine_parts(
+        combine, returned.reshape(experts * blocks, LANES), shared, peers
     )
-    centre, scale = moments(after, wide)
-    own = lax.dynamic_slice_in_dim(after, place * columns, columns, 1)
-    return ((own - centre) * scale * norm2_gain + norm2_bias).astype(jnp.bfloat16)
+    partials = exchanged(partial, "tp")
+    return finish(place, partials, whole, norm2_gain, norm2_bias, rows)
 
 
 def solution(mesh):

time: 129 us -> 94.1 us (0.73)
  blocking collectives: 38.3 us -> 7.76 us
  Pallas kernels: 29.4 us -> 10.3 us
  starting transfers between devices: 20.5 us -> 38.9 us
  local copies, waits for them, and re-layouts: 5.36 us -> 0.61 us
  other arithmetic: 1.72 us -> 3.18 us
    all_to_all x1, blocking collectives: 38.3 us -> 7.76 us  [exchanged(): return lax.all_to_all(blocks, axis, split_axis=0, concat_axis=0, tiled=True)]
    pallas_call x1 -> x5, Pallas kernels: 26.5 us -> 8.16 us  [the longest x1 5.05 us: stick_read(): pl.pallas_call(stick_kernel, out_shape=(jax.ShapeDtypeStruct((copies, PAD...]
    all_to_all x4, starting transfers between devices: 17.1 us -> 34.4 us  [exchanged(): return lax.all_to_all(blocks, axis, split_axis=0, concat_axis=0, tiled=True)]
    unnamed x32 -> x24, local copies, waits for them, and re-layouts: 3.63 us -> 0.24 us
    convert_element_type x3, other arithmetic: 0.89 us -> 2.95 us  [the longest x2 1.54 us: picks_of(): parts = (high.astype(jnp.bfloat16), (combine - high).astype(jnp.bfloat16))]
    broadcast_in_dim x2 -> x0, local copies, waits for them, and re-layouts: 1.34 us -> none  [the longest x1 0.7 us: body(): jnp.broadcast_to(partial, (peers, *partial.shape))]
  transfers between devices with their start and end apart: 5 -> 5, of which waited for: 4 -> 3; matrix products, arithmetic and copies ran while one was open for 3% -> 4% of each run, Pallas kernels for 0% -> 2%
where the time goes in v2:
time: 94.1 us; the launch traced here: 93.6 us
  starting transfers between devices  38.9 us (41%)
  waiting for transfers between devices  32.1 us (34%)
  Pallas kernels  10.3 us (11%)
  blocking collectives  7.76 us (8%)
  other arithmetic  3.18 us (3%)
    all_to_all x4, starting transfers between devices, exchanged(): return lax.all_to_all(blocks, axis, split_axis=0, concat_axis=0, tiled=True)  34.4 us
    all_to_all x4, waiting for transfers between devices, exchanged(): return lax.all_to_all(blocks, axis, split_axis=0, concat_axis=0, tiled=True)  32.1 us
    all_to_all x1, blocking collectives, exchanged(): return lax.all_to_all(blocks, axis, split_axis=0, concat_axis=0, tiled=True)  7.76 us
    pallas_call x1, Pallas kernels, stick_read(): pl.pallas_call(stick_kernel, out_shape=(jax.ShapeDtypeStruct((copies, PAD...  5.05 us
    ppermute x1, starting transfers between devices, body(): side = lax.ppermute(packed, ('ep', 'tp'), swaps)  4.57 us
    pallas_call x1, Pallas kernels, run_expert(): pl.pallas_call(expert_kernel, out_shape=jax.ShapeDtypeStruct(rows.shape,...  2.1 us
  transfers between devices with their start and end apart: 5, of which 3 were waited for; matrix products, arithmetic and copies ran while one was open for 4% of the time, Pallas kernels for 2%

profile of v2, /device:TPU:1, one launch (start us, length us, event | category | flops | bytes accessed | tf_op | source)
XLA Modules:
  0.0 93.6 jit_solution(6609986396437804271)
XLA Ops:
  0.0 0.0 copy-start
  0.0 0.0 copy-start.10
  0.0 0.0 copy-start.4
  0.0 0.0 copy-start.2
  0.0 0.0 copy-start.1
  0.0 5.1 %stick.1 = (bf16[4,8,512]{2,1,0:T(8,128)(2,1)}, bf16[3072,128]{1,0:T(8,128)(2,1)S(1)}) custom-call(s32[5]{0:T(128)} %lengths.1, f32[8]{0:T(128)} %offsets.1, bf16[5,512]{1,0:T(8,128)(2,1)} %queries.1, bf16[5,1024,128]{2,1,0:T(8,128)(2,1)} %keys.1, bf16[5,1024,128]{2,1,0:T(8,128)(2,1)} %values.1, bf16[1,1024,128]{2,1,0:T(8,128)(2,1)} %gate.1, ...), custom_call_target="tpu_custom_call" | custom-call | tf_op jit(solution)/shard_map/stick/pallas_call | solution.py:122
  5.1 0.0 copy-start.9
  5.1 4.8 %all-to-all-start = ((bf16[4,8,512]{2,1,0:T(8,128)(2,1)}), bf16[4,8,512]{2,1,0:T(8,128)(2,1)S(1)}, u32[]{:S(2)}, u32[]{:S(2)}) async-start(bf16[4,8,512]{2,1,0:T(8,128)(2,1)} %get-tuple-element.9), calls=%async_computation | async-start | bytes 65536 | tf_op jit(solution)/shard_map/all_to_all | solution.py:323
  10.0 4.6 %collective-permute-start = (bf16[3072,128]{1,0:T(8,128)(2,1)S(1)}, bf16[3072,128]{1,0:T(8,128)(2,1)S(1)}, u32[]{:S(2)}, u32[]{:S(2)}) collective-permute-start(bf16[3072,128]{1,0:T(8,128)(2,1)S(1)} %get-tuple-element.11.packed), channel_id=1, source_target_pairs={{0,1},{1,0},{2,3},{3,2},{4,7},{5,6},{6,5},{7,4},{8,9},{9,8},{10,11... | collective-permute-start | bytes 2359304 | tf_op jit(solution)/shard_map/ppermute | solution.py:397
  14.6 0.0 copy-done.10
  14.6 0.1 copy.26
  14.7 0.1 eq.144
  14.8 0.2 convert_reduce_fusion
  15.0 0.1 eq.150
  15.1 0.1 copy.29
  15.2 0.1 tile.9
  15.3 0.0 all-to-all-done
  15.3 0.0 copy-done.3
  15.3 0.0 copy-done.4
  15.4 0.0 copy-done.2
  15.4 0.0 copy-done.1
  15.4 0.9 project.1
  16.3 3.3 %all-to-all-start.1 = ((f32[4,24,256]{2,1,0:T(8,128)}), f32[4,24,256]{2,1,0:T(8,128)S(1)}, u32[]{:S(2)}, u32[]{:S(2)}) async-start(f32[4,24,256]{2,1,0:T(8,128)} %project.1), calls=%async_computation.1 | async-start | bytes 196608 | tf_op jit(solution)/shard_map/all_to_all | solution.py:323
  19.6 1.4 %add_convert_fusion.dispatch = bf16[1024,192]{1,0:T(8,128)(2,1)S(1)} fusion(s32[192]{0:T(256)S(1)} %bitcast.41, s32[192]{0:T(256)S(1)} %bitcast.44, s32[192]{0:T(256)S(1)} %bitcast.47, s32[192]{0:T(256)S(1)} %bitcast.50, s32[192]{0:T(256)S(1)} %bitcast.53, s32[1024]{0:T(1024)S(1)} %get-tuple-element.25, s32[1024]{0:T(1024)S(1)} %get-tuple-element.28, ...), kind=kLoop, calls=%fused_computation.5 | loop fusion | flops 4521984 | bytes 417984 | tf_op jit(solution)/shard_map/convert_element_type | solution.py:352
  21.0 3.7 %all-to-all-done.1.got = f32[4,24,256]{2,1,0:T(8,128)S(1)} async-done(((f32[4,24,256]{2,1,0:T(8,128)}), f32[4,24,256]{2,1,0:T(8,128)S(1)}, u32[]{:S(2)}, u32[]{:S(2)}) %all-to-all-start.1) | async-done | bytes 98336 | tf_op jit(solution)/shard_map/all_to_all | solution.py:323
  24.7 1.1 %norm.1 = (bf16[24,1024]{1,0:T(8,128)(2,1)S(1)}, bf16[1024,128]{1,0:T(8,128)(2,1)}) custom-call(f32[4,24,256]{2,1,0:T(8,128)S(1)} %all-to-all-done.1.got, bf16[1024,192]{1,0:T(8,128)(2,1)S(1)} %add_convert_fusion.dispatch), custom_call_target="tpu_custom_call" | custom-call | tf_op jit(solution)/shard_map/norm/pallas_call | solution.py:219
  25.8 20.7 %all-to-all-start.2 = ((bf16[128,8,128]{2,1,0:T(8,128)(2,1)}), bf16[128,8,128]{2,1,0:T(8,128)(2,1)S(1)}, u32[]{:S(2)}, u32[]{:S(2)}) async-start(bf16[128,8,128]{2,1,0:T(8,128)(2,1)} %bitcast.16), calls=%async_computation.2 | async-start | bytes 524288 | tf_op jit(solution)/shard_map/all_to_all | solution.py:323
  46.5 0.0 copy-done.9
  46.6 0.1 tile.21
  46.6 0.8 fusion.8.low
  47.4 14.3 %all-to-all-done.2 = bf16[128,8,128]{2,1,0:T(8,128)(2,1)S(1)} async-done(((bf16[128,8,128]{2,1,0:T(8,128)(2,1)}), bf16[128,8,128]{2,1,0:T(8,128)(2,1)S(1)}, u32[]{:S(2)}, u32[]{:S(2)}) %all-to-all-start.2) | async-done | bytes 262176 | tf_op jit(solution)/shard_map/all_to_all | solution.py:323
  61.8 0.0 collective-permute-done.side
  61.8 2.1 %expert.1 = bf16[1024,128]{1,0:T(8,128)(2,1)} custom-call(bf16[1024,128]{1,0:T(8,128)(2,1)S(1)} %bitcast.32, bf16[3072,128]{1,0:T(8,128)(2,1)S(1)} %get-tuple-element.11.packed, bf16[3072,128]{1,0:T(8,128)(2,1)S(1)} %collective-permute-done.side), custom_call_target="tpu_custom_call" | custom-call | tf_op jit(solution)/shard_map/expert/pallas_call | solution.py:258
  63.9 5.5 %all-to-all-start.3 = ((bf16[128,8,128]{2,1,0:T(8,128)(2,1)}), bf16[128,8,128]{2,1,0:T(8,128)(2,1)S(1)}, u32[]{:S(2)}, u32[]{:S(2)}) async-start(bf16[128,8,128]{2,1,0:T(8,128)(2,1)} %bitcast.18), calls=%async_computation.3 | async-start | bytes 524288 | tf_op jit(solution)/shard_map/all_to_all | solution.py:323
  69.4 0.7 reduce-precision_convert_fusion.high
  70.2 0.0 copy-done.7
  70.2 0.0 copy-start.5
  70.2 0.0 copy-start.6
  70.2 0.2 fusion.31
  70.4 0.0 copy-done
  70.4 0.0 copy-done.8
  70.4 0.3 fusion.1.shared
  70.7 14.1 %all-to-all-done.3 = bf16[128,8,128]{2,1,0:T(8,128)(2,1)S(1)} async-done(((bf16[128,8,128]{2,1,0:T(8,128)(2,1)}), bf16[128,8,128]{2,1,0:T(8,128)(2,1)S(1)}, u32[]{:S(2)}, u32[]{:S(2)}) %all-to-all-start.3) | async-done | bytes 262176 | tf_op jit(solution)/shard_map/all_to_all | solution.py:323
  84.8 0.4 combine.1
  85.1 7.8 %all_to_all.25.partials = bf16[4,24,1024]{2,1,0:T(8,128)(2,1)S(1)} all-to-all(bf16[4,24,1024]{2,1,0:T(8,128)(2,1)S(1)} %combine.1), channel_id=1, replica_groups=mesh['ep'=128,'tp'=4] {'tp'}, dimensions={0} | all-to-all | bytes 393216 | tf_op jit(solution)/shard_map/all_to_all | solution.py:323
  92.9 0.0 copy-done.5
  92.9 0.0 copy-done.6
  92.9 0.7 finish.1
  (16 shorter events, 0.1 us)
Async XLA Ops:
  0.0 70.4 %copy-start = (bf16[128,1024]{1,0:T(8,128)(2,1)S(1)}, bf16[128,1024]{1,0:T(8,128)(2,1)}, u32[]{:S(2)}) copy-start(bf16[128,1024]{1,0:T(8,128)(2,1)} %param.35) | copy-start | bytes 786436
  0.0 14.6 %copy-start.10 = (s32[20,6]{0,1:T(8,128)S(1)}, s32[20,6]{0,1:T(8,128)}, u32[]{:S(2)}) copy-start(s32[20,6]{0,1:T(8,128)} %param.28) | copy-start | bytes 1444
  0.0 15.3 %copy-start.3 = (f32[256]{0:T(256)S(1)}, f32[256]{0:T(256)}, u32[]{:S(2)}) copy-start(f32[256]{0:T(256)} %param.26) | copy-start | bytes 3076
  0.0 15.3 %copy-start.4 = (f32[256]{0:T(256)S(1)}, f32[256]{0:T(256)}, u32[]{:S(2)}) copy-start(f32[256]{0:T(256)} %param.27) | copy-start | bytes 3076
  0.0 15.3 %copy-start.2 = (bf16[20,256]{1,0:T(8,128)(2,1)S(1)}, bf16[20,256]{1,0:T(8,128)(2,1)}, u32[]{:S(2)}) copy-start(bf16[20,256]{1,0:T(8,128)(2,1)} %residual.1) | copy-start | bytes 30724
  0.0 15.3 %copy-start.1 = (bf16[512,256]{1,0:T(8,128)(2,1)S(1)}, bf16[512,256]{1,0:T(8,128)(2,1)}, u32[]{:S(2)}) copy-start(bf16[512,256]{1,0:T(8,128)(2,1)} %weight.1) | copy-start | bytes 786436
  5.1 41.4 %copy-start.9 = (f32[20,6]{0,1:T(8,128)S(1)}, f32[20,6]{0,1:T(8,128)}, u32[]{:S(2)}) copy-start(f32[20,6]{0,1:T(8,128)} %param.29) | copy-start | bytes 1444
  5.1 10.2 %all-to-all-start = ((bf16[4,8,512]{2,1,0:T(8,128)(2,1)}), bf16[4,8,512]{2,1,0:T(8,128)(2,1)S(1)}, u32[]{:S(2)}, u32[]{:S(2)}) async-start(bf16[4,8,512]{2,1,0:T(8,128)(2,1)} %get-tuple-element.9), calls=%async_computation | async-start | bytes 65536 | tf_op jit(solution)/shard_map/all_to_all | solution.py:323
  10.0 51.8 %collective-permute-start = (bf16[3072,128]{1,0:T(8,128)(2,1)S(1)}, bf16[3072,128]{1,0:T(8,128)(2,1)S(1)}, u32[]{:S(2)}, u32[]{:S(2)}) collective-permute-start(bf16[3072,128]{1,0:T(8,128)(2,1)S(1)} %get-tuple-element.11.packed), channel_id=1, source_target_pairs={{0,1},{1,0},{2,3},{3,2},{4,7},{5,6},{6,5},{7,4},{8,9},{9,8},{10,11... | collective-permute-start | bytes 2359304 | tf_op jit(solution)/shard_map/ppermute | solution.py:397
  16.3 8.5 %all-to-all-start.1 = ((f32[4,24,256]{2,1,0:T(8,128)}), f32[4,24,256]{2,1,0:T(8,128)S(1)}, u32[]{:S(2)}, u32[]{:S(2)}) async-start(f32[4,24,256]{2,1,0:T(8,128)} %project.1), calls=%async_computation.1 | async-start | bytes 196608 | tf_op jit(solution)/shard_map/all_to_all | solution.py:323
  25.8 35.9 %all-to-all-start.2 = ((bf16[128,8,128]{2,1,0:T(8,128)(2,1)}), bf16[128,8,128]{2,1,0:T(8,128)(2,1)S(1)}, u32[]{:S(2)}, u32[]{:S(2)}) async-start(bf16[128,8,128]{2,1,0:T(8,128)(2,1)} %bitcast.16), calls=%async_computation.2 | async-start | bytes 524288 | tf_op jit(solution)/shard_map/all_to_all | solution.py:323
  61.8 8.4 %copy-start.7 = (bf16[1024,128]{1,0:T(8,128)(2,1)S(1)}, bf16[1024,128]{1,0:T(8,128)(2,1)}, u32[]{:S(2)}) copy-start(bf16[1024,128]{1,0:T(8,128)(2,1)} %param.33) | copy-start | bytes 786436
  61.8 8.6 %copy-start.8 = (bf16[1024,128]{1,0:T(8,128)(2,1)S(1)}, bf16[1024,128]{1,0:T(8,128)(2,1)}, u32[]{:S(2)}) copy-start(bf16[1024,128]{1,0:T(8,128)(2,1)} %param.34) | copy-start | bytes 786436
  63.9 20.9 %all-to-all-start.3 = ((bf16[128,8,128]{2,1,0:T(8,128)(2,1)}), bf16[128,8,128]{2,1,0:T(8,128)(2,1)S(1)}, u32[]{:S(2)}, u32[]{:S(2)}) async-start(bf16[128,8,128]{2,1,0:T(8,128)(2,1)} %bitcast.18), calls=%async_computation.3 | async-start | bytes 524288 | tf_op jit(solution)/shard_map/all_to_all | solution.py:323
  70.2 22.7 %copy-start.5 = (f32[256]{0:T(256)S(1)}, f32[256]{0:T(256)}, u32[]{:S(2)}) copy-start(f32[256]{0:T(256)} %param.36) | copy-start | bytes 3076
  70.2 22.7 %copy-start.6 = (f32[256]{0:T(256)S(1)}, f32[256]{0:T(256)}, u32[]{:S(2)}) copy-start(f32[256]{0:T(256)} %param.37) | copy-start | bytes 3076

commit v3 on v2

--- a/solution.py
+++ b/solution.py
@@ -7,11 +7,11 @@
 from jax.experimental.pallas import tpu as pltpu
 from jax.sharding import PartitionSpec as P
 
+
 H = 8
 HD = 64
 KVH = 2
 CACHE = 1024
-TOPK = 6
 LANES = 128
 BLOCKS = CACHE // LANES
 PADDED = 8
@@ -143,17 +143,18 @@
     ))
 
 
-def project_kernel(reads, weight, residual, gain, bias, out):
-    sources, seqs = out.shape[0], residual.shape[0] // out.shape[0]
+def project_kernel(reads, weight, residual, gain, bias, dispatch, out, parcel):
     rows, columns = residual.shape
+    seqs = rows * PADDED // reads.shape[0]
     token = lax.broadcasted_iota(jnp.int32, (GROUP, reads.shape[0]), 0)
     arrived = lax.broadcasted_iota(jnp.int32, (GROUP, reads.shape[0]), 1)
-    held = jnp.zeros((GROUP, reads.shape[0]), jnp.bool_)
-    for t in range(sources):
+    held = jnp.zeros((GROUP, reads.shape[0]), jnp.float32)
+    for t in range(rows // seqs):
         inside = (token >= t * seqs) & (token < (t + 1) * seqs)
-        held = held | (inside & (arrived == token + t * (PADDED - seqs)))
-    held = jnp.where(held, 1.0, 0.0).astype(jnp.bfloat16)
-    mixed = jnp.dot(held, reads[...], preferred_element_type=jnp.float32).astype(jnp.bfloat16)
+        held = jnp.where(inside & (arrived == token + t * (PADDED - seqs)), 1.0, held)
+    mixed = jnp.dot(
+        held.astype(jnp.bfloat16), reads[...], preferred_element_type=jnp.float32
+    ).astype(jnp.bfloat16)
     pairs = H // KVH
     attended = jnp.zeros((GROUP, columns), jnp.float32)
     for h in range(pairs):
@@ -163,26 +164,32 @@
         attended = attended + jnp.dot(
             mixed[:, h * LANES : (h + 1) * LANES], part, preferred_element_type=jnp.float32
         )
-    before = RESIDUAL_SCALE * residual[...].astype(jnp.float32) + attended[0:rows]
-    rest = jnp.zeros((GROUP - rows - 2, columns), jnp.float32)
-    for d in range(sources):
-        out[d, 0:rows] = before
-        out[d, rows : rows + 1] = gain[...]
-        out[d, rows + 1 : rows + 2] = bias[...]
-        out[d, rows + 2 :] = rest
-
-
-def project(reads, weight, residual, gain, bias, copies):
+    out[0:rows] = RESIDUAL_SCALE * residual[...].astype(jnp.float32) + attended[0:rows]
+    out[rows : rows + 1] = gain[...]
+    out[rows + 1 : rows + 2] = bias[...]
+    out[rows + 2 :] = jnp.zeros((GROUP - rows - 2, columns), jnp.float32)
+    stacked = jnp.concatenate(
+        [out[:, j * LANES : (j + 1) * LANES] for j in range(columns // LANES)], axis=0
+    )
+    parcel[...] = jnp.dot(
+        dispatch[...], stacked.astype(jnp.bfloat16), preferred_element_type=jnp.float32
+    ).astype(jnp.bfloat16)
+
+
+def project(reads, weight, residual, gain, bias, dispatch):
     columns = weight.shape[1]
     vector = pl.BlockSpec(memory_space=pltpu.VMEM)
     return pl.pallas_call(
         project_kernel,
-        out_shape=jax.ShapeDtypeStruct((copies, GROUP, columns), jnp.float32),
-        in_specs=[vector] * 5,
-        out_specs=vector,
+        out_shape=(
+            jax.ShapeDtypeStruct((GROUP, columns), jnp.float32),
+            jax.ShapeDtypeStruct((dispatch.shape[0], LANES), jnp.bfloat16),
+        ),
+        in_specs=[vector] * 6,
+        out_specs=(vector, vector),
         compiler_params=GRANT,
         name="project",
-    )(reads, weight, residual, gain.reshape(1, -1), bias.reshape(1, -1))
+    )(reads, weight, residual, gain.reshape(1, -1), bias.reshape(1, -1), dispatch)
 
 
 def row_moments(blocks, entries):
@@ -196,46 +203,50 @@
     return centre, lax.rsqrt(spread + EPSILON)
 
 
-def norm_kernel(rows, got, dispatch, whole, parcel):
+def norm_kernel(rows, order, *refs):
+    pieces, (whole, affine) = refs[:-2], refs[-2:]
+    columns = pieces[0].shape[1]
     blocks = []
-    for t in range(got.shape[0]):
-        for j in range(got.shape[2] // LANES):
-            blocks.append(got[t, :, j * LANES : (j + 1) * LANES])
+    for piece in pieces:
+        for j in range(columns // LANES):
+            blocks.append(piece[:, j * LANES : (j + 1) * LANES])
     centre, scale = row_moments(blocks, len(blocks) * LANES)
-    normed = []
-    for j, block in enumerate(blocks):
-        value = (block - centre) * scale * block[rows : rows + 1] + block[rows + 1 : rows + 2]
-        normed.append(value)
-        whole[:, j * LANES : (j + 1) * LANES] = value.astype(jnp.bfloat16)
-    stacked = jnp.concatenate(normed, axis=0).astype(jnp.bfloat16)
-    parcel[...] = jnp.dot(
-        dispatch[...], stacked, preferred_element_type=jnp.float32
-    ).astype(jnp.bfloat16)
-
-
-def normalize_and_pick(got, dispatch, rows):
-    wide = got.shape[0] * got.shape[2]
+    for i, piece in enumerate(pieces):
+        at = pl.ds(pl.multiple_of(order[i] * columns, columns), columns)
+        gain, shift = piece[rows : rows + 1], piece[rows + 1 : rows + 2]
+        whole[:, at] = ((piece[...] - centre) * scale * gain + shift).astype(jnp.bfloat16)
+        affine[0:1, at] = gain
+        affine[1:2, at] = shift
+
+
+def normalize(pieces, order, rows):
+    wide = len(pieces) * pieces[0].shape[1]
     vector = pl.BlockSpec(memory_space=pltpu.VMEM)
     return pl.pallas_call(
         functools.partial(norm_kernel, rows),
         out_shape=(
             jax.ShapeDtypeStruct((GROUP, wide), jnp.bfloat16),
-            jax.ShapeDtypeStruct((dispatch.shape[0], LANES), jnp.bfloat16),
+            jax.ShapeDtypeStruct((2, wide), jnp.float32),
         ),
-        in_specs=[vector] * 2,
+        in_specs=[pl.BlockSpec(memory_space=pltpu.SMEM)] + [vector] * len(pieces),
         out_specs=(vector, vector),
         compiler_params=GRANT,
         name="norm",
-    )(got, dispatch)
-
-
-def expert_kernel(rows, packed, side, out, turned):
-    count, blocks = turned.shape[0], turned.shape[1]
+    )(order, *pieces)
+
+
+def expert_kernel(rows, affine, packed, side, out, turned):
+    blocks = turned.shape[1]
     wide, hidden = blocks * LANES, packed.shape[1]
     turned[...] = rows[...].astype(jnp.float32).reshape(turned.shape)
-    features = jnp.concatenate(
-        [turned[:, j, :].astype(jnp.bfloat16) for j in range(blocks)], axis=1
-    )
+    parts = [turned[:, j, :] for j in range(blocks)]
+    centre, scale = row_moments(parts, wide)
+    features = []
+    for j, part in enumerate(parts):
+        gain = affine[0:1, j * LANES : (j + 1) * LANES]
+        shift = affine[1:2, j * LANES : (j + 1) * LANES]
+        features.append(((part - centre) * scale * gain + shift).astype(jnp.bfloat16))
+    features = jnp.concatenate(features, axis=1)
 
     def silu_times(weights):
         gated = jnp.dot(features, weights[0:wide], preferred_element_type=jnp.float32)
@@ -252,18 +263,18 @@
     out[...] = turned[...].reshape(out.shape).astype(jnp.bfloat16)
 
 
-def run_expert(rows, packed, side, count):
+def run_expert(rows, affine, packed, side, count):
     blocks = rows.shape[0] // count
     vector = pl.BlockSpec(memory_space=pltpu.VMEM)
     return pl.pallas_call(
         expert_kernel,
         out_shape=jax.ShapeDtypeStruct(rows.shape, jnp.bfloat16),
-        in_specs=[vector] * 3,
+        in_specs=[vector] * 4,
         out_specs=vector,
         scratch_shapes=[pltpu.VMEM((count, blocks, LANES), jnp.float32)],
         compiler_params=GRANT,
         name="expert",
-    )(rows, packed, side)
+    )(rows, affine, packed, side)
 
 
 def combine_kernel(high, low, returned, shared, out):
@@ -328,28 +339,38 @@
     return jnp.pad(values, ((0, short), (0, 0)), constant_values=fill)
 
 
-def picks_of(routes, route_weights, mine, experts, blocks):
+def picks_of(routes, route_weights, mine, experts, peers, blocks):
     chosen = routes.reshape(-1)
     order = jnp.arange(chosen.shape[0])
     earlier = (chosen[:, None] == chosen[None, :]) & (order[None, :] < order[:, None])
     slots = jnp.sum(earlier.astype(jnp.int32), axis=1).reshape(routes.shape)
-    target = padded_rows(jnp.where(slots == mine, routes, -1), -1)
+    target = padded_rows(routes * 2 + slots, -1)
     weight = padded_rows(route_weights, 0.0)
+
+    pieces = blocks // peers
+    shape = (experts * blocks, pieces * GROUP)
+    row = lax.broadcasted_iota(jnp.int32, shape, 0)
+    piece = lax.broadcasted_iota(jnp.int32, shape, 1) // GROUP
+    wanted = row // blocks * 2 + row // pieces % 2
+    wanted = jnp.where(row % pieces == piece, wanted, -2)
+    turned = jnp.tile(target.T, (1, pieces))
+    picked = jnp.zeros(shape, jnp.float32)
+    for k in range(routes.shape[1]):
+        picked = picked + jnp.where(turned[k : k + 1] == wanted, 1.0, 0.0)
+
     target = jnp.tile(target, (blocks, 1))
     weight = jnp.tile(weight, (blocks, 1))
     shape = (blocks * GROUP, experts * blocks)
     block = lax.broadcasted_iota(jnp.int32, shape, 0) // GROUP
     column = lax.broadcasted_iota(jnp.int32, shape, 1)
-    expert = jnp.where(column % blocks == block, column // blocks, -2)
-    picked = jnp.zeros(shape, jnp.float32)
+    wanted = jnp.where(column % blocks == block, column // blocks * 2 + mine, -2)
     combine = jnp.zeros(shape, jnp.float32)
     for k in range(routes.shape[1]):
-        hit = target[:, k : k + 1] == expert
-        picked = picked + jnp.where(hit, 1.0, 0.0)
+        hit = target[:, k : k + 1] == wanted
         combine = combine + jnp.where(hit, weight[:, k : k + 1], 0.0)
     high = lax.reduce_precision(combine, 8, 7)
     parts = (high.astype(jnp.bfloat16), (combine - high).astype(jnp.bfloat16))
-    return picked.T.astype(jnp.bfloat16), parts
+    return picked.astype(jnp.bfloat16), parts
 
 
 def body(
@@ -385,9 +406,12 @@
         expert_gate, expert_up, expert_down, peers,
     )
     reads = exchanged(mixed, "tp").reshape(peers * PADDED, H * HD)
-    dispatch, combine = picks_of(routes, route_weights, place % 2, experts, blocks)
-    sent = project(reads, out_weight, residual_in, norm1_gain, norm1_bias, peers)
-    got = exchanged(sent, "tp")
+    dispatch, combine = picks_of(routes, route_weights, place % 2, experts, peers, blocks)
+    sent, parcel = project(
+        reads, out_weight, residual_in, norm1_gain, norm1_bias, dispatch
+    )
+    parcel = parcel.reshape(experts * peers, blocks // peers, LANES)
+    arrived = exchanged(parcel, ("ep", "tp")).reshape(experts * blocks, LANES)
 
     swaps = []
     for e in range(experts):
@@ -395,10 +419,12 @@
             partner = t ^ 1 if e % 2 == 0 else ((t + 1) ^ 1) - 1
             swaps.append((e * peers + t, e * peers + partner % peers))
     side = lax.ppermute(packed, ("ep", "tp"), swaps)
-
-    whole, parcel = normalize_and_pick(got, dispatch, rows)
-    arrived = exchanged(parcel.reshape(experts, blocks, LANES), "ep")
-    produced = run_expert(arrived.reshape(experts * blocks, LANES), packed, side, experts)
+    pieces = [sent]
+    for k in range(1, peers):
+        pieces.append(lax.ppermute(sent, "tp", [(i, (i + k) % peers) for i in range(peers)]))
+    order = (place - jnp.arange(peers, dtype=jnp.int32)) % peers
+    whole, affine = normalize(pieces, order, rows)
+    produced = run_expert(arrived, affine, packed, side, experts)
     returned = exchanged(produced.reshape(experts, blocks, LANES), "ep")
     shared_hidden = (
         jax.nn.silu(jnp.dot(whole, shared_gate, preferred_element_type=jnp.float32))
@@ -435,4 +461,5 @@
         P("tp"),
     )
     out_specs = P("ep", "tp")
+
     return jax.shard_map(body, mesh=mesh, in_specs=in_specs, out_specs=out_specs, check_vma=False)

time: 94.1 us -> 98.7 us (1.049)
  starting transfers between devices: 38.9 us -> 55.1 us
  waiting for transfers between devices: 32.1 us -> 18.3 us
    all_to_all x4 -> x3, waiting for transfers between devices: 32.1 us -> 16.5 us  [exchanged(): return lax.all_to_all(blocks, axis, split_axis=0, concat_axis=0, tiled=True)]
    ppermute x0 -> x3, starting transfers between devices: none -> 10.7 us  [body(): lax.ppermute(sent, 'tp', [(i, (i + k) % peers) for i in range(peers)])]
    all_to_all x4 -> x3, starting transfers between devices: 34.4 us -> 39.9 us  [exchanged(): return lax.all_to_all(blocks, axis, split_axis=0, concat_axis=0, tiled=True)]
    ppermute x0 -> x3, waiting for transfers between devices: none -> 1.78 us  [body(): lax.ppermute(sent, 'tp', [(i, (i + k) % peers) for i in range(peers)])]
  transfers between devices with their start and end apart: 5 -> 7, of which waited for: 3 -> 3; matrix products, arithmetic and copies ran while one was open for 4% -> 5% of each run, Pallas kernels for 2% -> 2%
where the time goes in v3:
time: 98.7 us; the launch traced here: 98.3 us
  starting transfers between devices  55.1 us (56%)
  waiting for transfers between devices  18.3 us (19%)
  Pallas kernels  10.5 us (11%)
  blocking collectives  8.72 us (9%)
  other arithmetic  3.52 us (4%)
  local copies, waits for them, and re-layouts  1.38 us (1%)
    all_to_all x3, starting transfers between devices, exchanged(): return lax.all_to_all(blocks, axis, split_axis=0, concat_axis=0, tiled=True)  39.9 us
    all_to_all x3, waiting for transfers between devices, exchanged(): return lax.all_to_all(blocks, axis, split_axis=0, concat_axis=0, tiled=True)  16.5 us
    ppermute x3, starting transfers between devices, body(): lax.ppermute(sent, 'tp', [(i, (i + k) % peers) for i in range(peers)])  10.7 us
    all_to_all x1, blocking collectives, exchanged(): return lax.all_to_all(blocks, axis, split_axis=0, concat_axis=0, tiled=True)  8.72 us
    pallas_call x1, Pallas kernels, stick_read(): pl.pallas_call(stick_kernel, out_shape=(jax.ShapeDtypeStruct((copies, PAD...  5.06 us
    ppermute x1, starting transfers between devices, body(): side = lax.ppermute(packed, ('ep', 'tp'), swaps)  4.57 us
    pallas_call x1, Pallas kernels, run_expert(): pl.pallas_call(expert_kernel, out_shape=jax.ShapeDtypeStruct(rows.shape,...  2.44 us
  transfers between devices with their start and end apart: 7, of which 3 were waited for; matrix products, arithmetic and copies ran while one was open for 5% of the time, Pallas kernels for 2%

profile of v3, /device:TPU:1, one launch (start us, length us, event | category | flops | bytes accessed | tf_op | source)
XLA Modules:
  0.0 98.3 jit_solution(3085280790323224785)
XLA Ops:
  0.0 0.0 copy-start
  0.1 5.1 %stick.1 = (bf16[4,8,512]{2,1,0:T(8,128)(2,1)}, bf16[3072,128]{1,0:T(8,128)(2,1)S(1)}) custom-call(s32[5]{0:T(128)} %lengths.1, f32[8]{0:T(128)} %offsets.1, bf16[5,512]{1,0:T(8,128)(2,1)} %queries.1, bf16[5,1024,128]{2,1,0:T(8,128)(2,1)} %keys.1, bf16[5,1024,128]{2,1,0:T(8,128)(2,1)} %values.1, bf16[1,1024,128]{2,1,0:T(8,128)(2,1)} %gate.1, ...), custom_call_target="tpu_custom_call" | custom-call | tf_op jit(solution)/shard_map/stick/pallas_call | solution.py:122
  5.1 4.8 %all-to-all-start = ((bf16[4,8,512]{2,1,0:T(8,128)(2,1)}), bf16[4,8,512]{2,1,0:T(8,128)(2,1)S(1)}, u32[]{:S(2)}, u32[]{:S(2)}) async-start(bf16[4,8,512]{2,1,0:T(8,128)(2,1)} %get-tuple-element.11), calls=%async_computation | async-start | bytes 65536 | tf_op jit(solution)/shard_map/all_to_all | solution.py:334
  10.0 4.6 %collective-permute-start.3 = (bf16[3072,128]{1,0:T(8,128)(2,1)S(1)}, bf16[3072,128]{1,0:T(8,128)(2,1)S(1)}, u32[]{:S(2)}, u32[]{:S(2)}) collective-permute-start(bf16[3072,128]{1,0:T(8,128)(2,1)S(1)} %get-tuple-element.15.packed), channel_id=1, source_target_pairs={{0,1},{1,0},{2,3},{3,2},{4,7},{5,6},{6,5},{7,4},{8,9},{9,8},{10,11... | collective-permute-start | bytes 2359304 | tf_op jit(solution)/shard_map/ppermute | solution.py:421
  14.6 0.1 copy.26
  14.7 0.1 eq.148
  14.8 0.2 convert_reduce_fusion
  15.0 0.1 reshape.71
  15.1 0.1 copy.29
  15.2 0.3 slice_reduce_fusion.5
  15.5 0.1 tile.52
  15.6 0.1 tile.54
  15.7 0.1 tile.56
  15.8 0.1 tile.58
  15.8 0.1 tile.60
  15.9 0.1 tile.62
  16.0 0.1 tile.48
  16.1 0.0 copy-done.9
  16.1 0.1 tile.50
  16.2 1.7 %add_convert_fusion.dispatch = bf16[1024,48]{1,0:T(8,128)(2,1)S(1)} fusion(s32[48]{0:T(128)S(1)} %tile.62, s32[48]{0:T(128)S(1)} %tile.60, s32[48]{0:T(128)S(1)} %tile.58, s32[48]{0:T(128)S(1)} %tile.56, s32[48]{0:T(128)S(1)} %tile.54, s32[1024]{0:T(1024)S(1)} %get-tuple-element.41, s32[1024]{0:T(1024)S(1)} %get-tuple-element.44, ...), kind=kLoop, calls=%fused_computation.20 | loop fusion | flops 1818624 | bytes 127536 | tf_op jit(solution)/shard_map/convert_element_type | solution.py:373
  18.0 0.0 all-to-all-done
  18.0 1.2 %project.1 = (f32[24,256]{1,0:T(8,128)S(1)}, bf16[1024,128]{1,0:T(8,128)(2,1)}) custom-call(bf16[32,512]{1,0:T(8,128)(2,1)S(1)} %bitcast.35, bf16[512,256]{1,0:T(8,128)(2,1)S(1)} %copy-done.1, bf16[20,256]{1,0:T(8,128)(2,1)S(1)} %copy-done.2, f32[1,256]{1,0:T(1,128)S(1)} %bitcast.36, f32[1,256]{1,0:T(1,128)S(1)} %bitcast.37, ...), custom_call_target="tpu_custom_call" | custom-call | tf_op jit(solution)/shard_map/project/pallas_call | solution.py:182
  19.3 20.6 %all-to-all-start.1 = ((bf16[512,2,128]{2,1,0:T(2,128)(2,1)}), bf16[512,2,128]{2,1,0:T(2,128)(2,1)S(1)}, u32[]{:S(2)}, u32[]{:S(2)}) async-start(bf16[512,2,128]{2,1,0:T(2,128)(2,1)} %bitcast.17), calls=%async_computation.1 | async-start | bytes 524288 | tf_op jit(solution)/shard_map/all_to_all | solution.py:334
  39.9 0.8 fusion.low
  40.7 3.3 %collective-permute-start = (f32[24,256]{1,0:T(8,128)S(1)}, f32[24,256]{1,0:T(8,128)S(1)}, u32[]{:S(2)}, u32[]{:S(2)}) collective-permute-start(f32[24,256]{1,0:T(8,128)S(1)} %get-tuple-element.13.refs_0_), channel_id=1, source_target_pairs={{0,1},{1,2},{2,3},{3,0},{4,5},{5,6},{6,7},{7,4},{8,9},{9,10},{10,1... | collective-permute-start | bytes 73736 | tf_op jit(solution)/shard_map/ppermute | solution.py:424
  44.0 4.3 %collective-permute-start.1 = (f32[24,256]{1,0:T(8,128)S(1)}, f32[24,256]{1,0:T(8,128)S(1)}, u32[]{:S(2)}, u32[]{:S(2)}) collective-permute-start(f32[24,256]{1,0:T(8,128)S(1)} %get-tuple-element.13.refs_0_), channel_id=1, source_target_pairs={{0,2},{1,3},{2,0},{3,1},{4,6},{5,7},{6,4},{7,5},{8,10},{9,11},{10,... | collective-permute-start | bytes 73736 | tf_op jit(solution)/shard_map/ppermute | solution.py:424
  48.3 3.1 %collective-permute-start.2 = (f32[24,256]{1,0:T(8,128)S(1)}, f32[24,256]{1,0:T(8,128)S(1)}, u32[]{:S(2)}, u32[]{:S(2)}) collective-permute-start(f32[24,256]{1,0:T(8,128)S(1)} %get-tuple-element.13.refs_0_), channel_id=1, source_target_pairs={{0,3},{1,0},{2,1},{3,2},{4,7},{5,4},{6,5},{7,6},{8,11},{9,8},{10,9... | collective-permute-start | bytes 73736 | tf_op jit(solution)/shard_map/ppermute | solution.py:424
  51.4 0.0 collective-permute-done.refs_1_
  51.4 0.0 collective-permute-done.1.refs_2_
  51.4 1.8 %collective-permute-done.2.refs_3_ = f32[24,256]{1,0:T(8,128)S(1)} collective-permute-done((f32[24,256]{1,0:T(8,128)S(1)}, f32[24,256]{1,0:T(8,128)S(1)}, u32[]{:S(2)}, u32[]{:S(2)}) %collective-permute-start.2) | collective-permute-done | bytes 24608 | tf_op jit(solution)/shard_map/ppermute | solution.py:424
  53.2 0.6 norm.1
  53.9 2.5 %all-to-all-done.1 = bf16[512,2,128]{2,1,0:T(2,128)(2,1)S(1)} async-done(((bf16[512,2,128]{2,1,0:T(2,128)(2,1)}), bf16[512,2,128]{2,1,0:T(2,128)(2,1)S(1)}, u32[]{:S(2)}, u32[]{:S(2)}) %all-to-all-start.1) | async-done | bytes 262176 | tf_op jit(solution)/shard_map/all_to_all | solution.py:334
  56.3 0.0 collective-permute-done.3.side
  56.4 2.4 %expert.1 = bf16[1024,128]{1,0:T(8,128)(2,1)} custom-call(bf16[1024,128]{1,0:T(8,128)(2,1)S(1)} %bitcast.34, f32[2,1024]{1,0:T(2,128)S(1)} %get-tuple-element.14.affine, bf16[3072,128]{1,0:T(8,128)(2,1)S(1)} %get-tuple-element.15.packed, bf16[3072,128]{1,0:T(8,128)(2,1)S(1)} %collective-permute-done.3.side), custom_call_target="tpu_custom_call" | custom-call | tf_op jit(solution)/shard_map/expert/pallas_call | solution.py:269
  58.8 14.4 %all-to-all-start.2 = ((bf16[128,8,128]{2,1,0:T(8,128)(2,1)}), bf16[128,8,128]{2,1,0:T(8,128)(2,1)S(1)}, u32[]{:S(2)}, u32[]{:S(2)}) async-start(bf16[128,8,128]{2,1,0:T(8,128)(2,1)} %bitcast.19), calls=%async_computation.2 | async-start | bytes 524288 | tf_op jit(solution)/shard_map/all_to_all | solution.py:334
  73.2 0.7 reduce-precision_convert_fusion.high
  74.0 0.0 copy-done.7
  74.0 0.0 copy-start.5
  74.0 0.0 copy-start.6
  74.0 0.2 fusion.30
  74.2 0.0 copy-done
  74.2 0.0 copy-done.8
  74.2 0.3 fusion.11.shared
  74.5 14.0 %all-to-all-done.2 = bf16[128,8,128]{2,1,0:T(8,128)(2,1)S(1)} async-done(((bf16[128,8,128]{2,1,0:T(8,128)(2,1)}), bf16[128,8,128]{2,1,0:T(8,128)(2,1)S(1)}, u32[]{:S(2)}, u32[]{:S(2)}) %all-to-all-start.2) | async-done | bytes 262176 | tf_op jit(solution)/shard_map/all_to_all | solution.py:334
  88.5 0.4 combine.1
  88.8 8.7 %all_to_all.20.partials = bf16[4,24,1024]{2,1,0:T(8,128)(2,1)S(1)} all-to-all(bf16[4,24,1024]{2,1,0:T(8,128)(2,1)S(1)} %combine.1), channel_id=1, replica_groups=mesh['ep'=128,'tp'=4] {'tp'}, dimensions={0} | all-to-all | bytes 393216 | tf_op jit(solution)/shard_map/all_to_all | solution.py:334
  97.6 0.0 copy-done.6
  97.6 0.7 finish.1
  (40 shorter events, 0.2 us)
Async XLA Ops:
  0.0 74.2 %copy-start = (bf16[128,1024]{1,0:T(8,128)(2,1)S(1)}, bf16[128,1024]{1,0:T(8,128)(2,1)}, u32[]{:S(2)}) copy-start(bf16[128,1024]{1,0:T(8,128)(2,1)} %param.35) | copy-start | bytes 786436
  0.0 14.6 %copy-start.10 = (s32[20,6]{0,1:T(8,128)S(1)}, s32[20,6]{0,1:T(8,128)}, u32[]{:S(2)}) copy-start(s32[20,6]{0,1:T(8,128)} %param.28) | copy-start | bytes 1444
  0.0 16.1 %copy-start.9 = (f32[20,6]{0,1:T(8,128)S(1)}, f32[20,6]{0,1:T(8,128)}, u32[]{:S(2)}) copy-start(f32[20,6]{0,1:T(8,128)} %param.29) | copy-start | bytes 1444
  0.0 18.0 %copy-start.3 = (f32[256]{0:T(256)S(1)}, f32[256]{0:T(256)}, u32[]{:S(2)}) copy-start(f32[256]{0:T(256)} %param.26) | copy-start | bytes 3076
  0.0 18.0 %copy-start.4 = (f32[256]{0:T(256)S(1)}, f32[256]{0:T(256)}, u32[]{:S(2)}) copy-start(f32[256]{0:T(256)} %param.27) | copy-start | bytes 3076
  0.0 18.0 %copy-start.2 = (bf16[20,256]{1,0:T(8,128)(2,1)S(1)}, bf16[20,256]{1,0:T(8,128)(2,1)}, u32[]{:S(2)}) copy-start(bf16[20,256]{1,0:T(8,128)(2,1)} %residual.1) | copy-start | bytes 30724
  0.0 18.0 %copy-start.1 = (bf16[512,256]{1,0:T(8,128)(2,1)S(1)}, bf16[512,256]{1,0:T(8,128)(2,1)}, u32[]{:S(2)}) copy-start(bf16[512,256]{1,0:T(8,128)(2,1)} %weight.1) | copy-start | bytes 786436
  5.1 12.9 %all-to-all-start = ((bf16[4,8,512]{2,1,0:T(8,128)(2,1)}), bf16[4,8,512]{2,1,0:T(8,128)(2,1)S(1)}, u32[]{:S(2)}, u32[]{:S(2)}) async-start(bf16[4,8,512]{2,1,0:T(8,128)(2,1)} %get-tuple-element.11), calls=%async_computation | async-start | bytes 65536 | tf_op jit(solution)/shard_map/all_to_all | solution.py:334
  10.0 46.4 %collective-permute-start.3 = (bf16[3072,128]{1,0:T(8,128)(2,1)S(1)}, bf16[3072,128]{1,0:T(8,128)(2,1)S(1)}, u32[]{:S(2)}, u32[]{:S(2)}) collective-permute-start(bf16[3072,128]{1,0:T(8,128)(2,1)S(1)} %get-tuple-element.15.packed), channel_id=1, source_target_pairs={{0,1},{1,0},{2,3},{3,2},{4,7},{5,6},{6,5},{7,4},{8,9},{9,8},{10,11... | collective-permute-start | bytes 2359304 | tf_op jit(solution)/shard_map/ppermute | solution.py:421
  19.3 37.1 %all-to-all-start.1 = ((bf16[512,2,128]{2,1,0:T(2,128)(2,1)}), bf16[512,2,128]{2,1,0:T(2,128)(2,1)S(1)}, u32[]{:S(2)}, u32[]{:S(2)}) async-start(bf16[512,2,128]{2,1,0:T(2,128)(2,1)} %bitcast.17), calls=%async_computation.1 | async-start | bytes 524288 | tf_op jit(solution)/shard_map/all_to_all | solution.py:334
  40.7 10.7 %collective-permute-start = (f32[24,256]{1,0:T(8,128)S(1)}, f32[24,256]{1,0:T(8,128)S(1)}, u32[]{:S(2)}, u32[]{:S(2)}) collective-permute-start(f32[24,256]{1,0:T(8,128)S(1)} %get-tuple-element.13.refs_0_), channel_id=1, source_target_pairs={{0,1},{1,2},{2,3},{3,0},{4,5},{5,6},{6,7},{7,4},{8,9},{9,10},{10,1... | collective-permute-start | bytes 73736 | tf_op jit(solution)/shard_map/ppermute | solution.py:424
  44.0 7.4 %collective-permute-start.1 = (f32[24,256]{1,0:T(8,128)S(1)}, f32[24,256]{1,0:T(8,128)S(1)}, u32[]{:S(2)}, u32[]{:S(2)}) collective-permute-start(f32[24,256]{1,0:T(8,128)S(1)} %get-tuple-element.13.refs_0_), channel_id=1, source_target_pairs={{0,2},{1,3},{2,0},{3,1},{4,6},{5,7},{6,4},{7,5},{8,10},{9,11},{10,... | collective-permute-start | bytes 73736 | tf_op jit(solution)/shard_map/ppermute | solution.py:424
  48.3 4.9 %collective-permute-start.2 = (f32[24,256]{1,0:T(8,128)S(1)}, f32[24,256]{1,0:T(8,128)S(1)}, u32[]{:S(2)}, u32[]{:S(2)}) collective-permute-start(f32[24,256]{1,0:T(8,128)S(1)} %get-tuple-element.13.refs_0_), channel_id=1, source_target_pairs={{0,3},{1,0},{2,1},{3,2},{4,7},{5,4},{6,5},{7,6},{8,11},{9,8},{10,9... | collective-permute-start | bytes 73736 | tf_op jit(solution)/shard_map/ppermute | solution.py:424
  56.3 17.6 %copy-start.7 = (bf16[1024,128]{1,0:T(8,128)(2,1)S(1)}, bf16[1024,128]{1,0:T(8,128)(2,1)}, u32[]{:S(2)}) copy-start(bf16[1024,128]{1,0:T(8,128)(2,1)} %param.33) | copy-start | bytes 786436
  56.3 17.8 %copy-start.8 = (bf16[1024,128]{1,0:T(8,128)(2,1)S(1)}, bf16[1024,128]{1,0:T(8,128)(2,1)}, u32[]{:S(2)}) copy-start(bf16[1024,128]{1,0:T(8,128)(2,1)} %param.34) | copy-start | bytes 786436
  58.8 29.7 %all-to-all-start.2 = ((bf16[128,8,128]{2,1,0:T(8,128)(2,1)}), bf16[128,8,128]{2,1,0:T(8,128)(2,1)S(1)}, u32[]{:S(2)}, u32[]{:S(2)}) async-start(bf16[128,8,128]{2,1,0:T(8,128)(2,1)} %bitcast.19), calls=%async_computation.2 | async-start | bytes 524288 | tf_op jit(solution)/shard_map/all_to_all | solution.py:334
  74.0 23.6 %copy-start.5 = (f32[256]{0:T(256)S(1)}, f32[256]{0:T(256)}, u32[]{:S(2)}) copy-start(f32[256]{0:T(256)} %param.36) | copy-start | bytes 3076
  74.0 23.6 %copy-start.6 = (f32[256]{0:T(256)S(1)}, f32[256]{0:T(256)}, u32[]{:S(2)}) copy-start(f32[256]{0:T(256)} %param.37) | copy-start | bytes 3076

commit v4 on v2

--- a/solution.py
+++ b/solution.py
@@ -7,11 +7,11 @@
 from jax.experimental.pallas import tpu as pltpu
 from jax.sharding import PartitionSpec as P
 
+
 H = 8
 HD = 64
 KVH = 2
 CACHE = 1024
-TOPK = 6
 LANES = 128
 BLOCKS = CACHE // LANES
 PADDED = 8
@@ -23,10 +23,11 @@
 
 
 def stick_kernel(
-    lengths, offsets, queries, keys, values, gate, up, down,
-    out, packed, keys_vm, values_vm, reads, key_sems, value_sems, pack_sems,
+    lengths_at, offsets_at, queries_at, keys, values, gate, up, down,
+    out, packed, lengths, offsets, queries, keys_vm, values_vm, reads,
+    small_sems, key_sems, value_sems, pack_sems,
 ):
-    seqs = queries.shape[0]
+    seqs = keys.shape[0]
     wide, hidden = gate.shape[1], gate.shape[2]
     key_copies = [
         pltpu.make_async_copy(keys.at[s], keys_vm.at[s], key_sems.at[s]) for s in range(seqs)
@@ -43,8 +44,16 @@
         pltpu.make_async_copy(piece, packed.at[pl.ds(at, rows)], pack_sems.at[i])
         for i, (piece, at, rows) in enumerate(pieces)
     ]
-    for copy in key_copies + value_copies + pack_copies:
+    small_copies = [
+        pltpu.make_async_copy(source, target, small_sems.at[i])
+        for i, (source, target) in enumerate(
+            ((queries_at, queries), (lengths_at, lengths), (offsets_at, offsets))
+        )
+    ]
+    for copy in small_copies + key_copies + value_copies + pack_copies:
         copy.start()
+    for copy in small_copies:
+        copy.wait()
 
     row = lax.broadcasted_iota(jnp.int32, (H, LANES), 0)
     lane = lax.broadcasted_iota(jnp.int32, (H, LANES), 1)
@@ -98,13 +107,20 @@
             weights[s][b] = jnp.exp(takes[s][b] + after)
             beyond = beyond + sums[at : at + H, LANES:]
 
-    for s in range(seqs):
-        stick = jnp.concatenate(weights[s], axis=1).astype(jnp.bfloat16)
-        value_copies[s].wait()
-        mixed = jnp.dot(stick, values_vm[s], preferred_element_type=jnp.float32)
-        mixed = jnp.where(low, mixed, pltpu.roll(mixed, H // KVH, 0))
-        for h in range(H // KVH):
-            reads[s : s + 1, h * LANES : (h + 1) * LANES] = mixed[h : h + 1, :]
+    for first_seq in range(0, seqs, 2):
+        pair = range(first_seq, min(first_seq + 2, seqs))
+        stick = jnp.concatenate(
+            [jnp.concatenate(weights[s], axis=1) for s in pair], axis=0
+        ).astype(jnp.bfloat16)
+        for s in pair:
+            value_copies[s].wait()
+        both = jnp.concatenate([values_vm[s] for s in pair], axis=1)
+        product = jnp.dot(stick, both, preferred_element_type=jnp.float32)
+        for i, s in enumerate(pair):
+            mixed = product[i * H : (i + 1) * H, i * LANES : (i + 1) * LANES]
+            mixed = jnp.where(low, mixed, pltpu.roll(mixed, H // KVH, 0))
+            for h in range(H // KVH):
+                reads[s : s + 1, h * LANES : (h + 1) * LANES] = mixed[h : h + 1, :]
     reads[seqs:, :] = jnp.zeros((reads.shape[0] - seqs, H * HD), jnp.float32)
     done = reads[...].astype(jnp.bfloat16)
     for d in range(out.shape[0]):
@@ -117,7 +133,6 @@
     seqs = queries.shape[0]
     wide, hidden = gate.shape[1], gate.shape[2]
     anywhere = pl.BlockSpec(memory_space=pltpu.HBM)
-    scalars = pl.BlockSpec(memory_space=pltpu.SMEM)
     vector = pl.BlockSpec(memory_space=pltpu.VMEM)
     return pl.pallas_call(
         stick_kernel,
@@ -125,12 +140,16 @@
             jax.ShapeDtypeStruct((copies, PADDED, H * HD), jnp.bfloat16),
             jax.ShapeDtypeStruct((3 * wide, hidden), jnp.bfloat16),
         ),
-        in_specs=[scalars, scalars, vector] + [anywhere] * 5,
+        in_specs=[anywhere] * 8,
         out_specs=(vector, vector),
         scratch_shapes=[
+            pltpu.SMEM(lengths.shape, jnp.int32),
+            pltpu.SMEM(offsets.shape, jnp.float32),
+            pltpu.VMEM(queries.shape, jnp.bfloat16),
             pltpu.VMEM(keys.shape, jnp.bfloat16),
             pltpu.VMEM(values.shape, jnp.bfloat16),
             pltpu.VMEM((PADDED, H * HD), jnp.float32),
+            pltpu.SemaphoreType.DMA((3,)),
             pltpu.SemaphoreType.DMA((seqs,)),
             pltpu.SemaphoreType.DMA((seqs,)),
             pltpu.SemaphoreType.DMA((2 + wide // LANES,)),
@@ -146,24 +165,21 @@
 def project_kernel(reads, weight, residual, gain, bias, out):
     sources, seqs = out.shape[0], residual.shape[0] // out.shape[0]
     rows, columns = residual.shape
-    token = lax.broadcasted_iota(jnp.int32, (GROUP, reads.shape[0]), 0)
-    arrived = lax.broadcasted_iota(jnp.int32, (GROUP, reads.shape[0]), 1)
-    held = jnp.zeros((GROUP, reads.shape[0]), jnp.bool_)
-    for t in range(sources):
-        inside = (token >= t * seqs) & (token < (t + 1) * seqs)
-        held = held | (inside & (arrived == token + t * (PADDED - seqs)))
-    held = jnp.where(held, 1.0, 0.0).astype(jnp.bfloat16)
-    mixed = jnp.dot(held, reads[...], preferred_element_type=jnp.float32).astype(jnp.bfloat16)
+    mixed = reads[...]
     pairs = H // KVH
-    attended = jnp.zeros((GROUP, columns), jnp.float32)
+    parts = []
     for h in range(pairs):
         part = jnp.concatenate(
             [weight[h * HD : (h + 1) * HD], weight[(pairs + h) * HD : (pairs + h + 1) * HD]], axis=0
         )
-        attended = attended + jnp.dot(
-            mixed[:, h * LANES : (h + 1) * LANES], part, preferred_element_type=jnp.float32
-        )
-    before = RESIDUAL_SCALE * residual[...].astype(jnp.float32) + attended[0:rows]
+        parts.append(part)
+    attended = jnp.dot(
+        mixed, jnp.concatenate(parts, axis=0), preferred_element_type=jnp.float32
+    )
+    attended = jnp.concatenate(
+        [attended[t * PADDED : t * PADDED + seqs] for t in range(sources)], axis=0
+    )
+    before = RESIDUAL_SCALE * residual[...].astype(jnp.float32) + attended
     rest = jnp.zeros((GROUP - rows - 2, columns), jnp.float32)
     for d in range(sources):
         out[d, 0:rows] = before
@@ -202,15 +218,14 @@
         for j in range(got.shape[2] // LANES):
             blocks.append(got[t, :, j * LANES : (j + 1) * LANES])
     centre, scale = row_moments(blocks, len(blocks) * LANES)
-    normed = []
-    for j, block in enumerate(blocks):
-        value = (block - centre) * scale * block[rows : rows + 1] + block[rows + 1 : rows + 2]
-        normed.append(value)
-        whole[:, j * LANES : (j + 1) * LANES] = value.astype(jnp.bfloat16)
-    stacked = jnp.concatenate(normed, axis=0).astype(jnp.bfloat16)
-    parcel[...] = jnp.dot(
-        dispatch[...], stacked, preferred_element_type=jnp.float32
-    ).astype(jnp.bfloat16)
+    normed = [
+        ((block - centre) * scale * block[rows : rows + 1] + block[rows + 1 : rows + 2])
+        for block in blocks
+    ]
+    normed = jnp.concatenate(normed, axis=1).astype(jnp.bfloat16)
+    whole[...] = normed
+    picked = jnp.dot(dispatch[...], normed, preferred_element_type=jnp.float32)
+    parcel[...] = picked.astype(jnp.bfloat16).reshape(parcel.shape)
 
 
 def normalize_and_pick(got, dispatch, rows):
@@ -220,7 +235,7 @@
         functools.partial(norm_kernel, rows),
         out_shape=(
             jax.ShapeDtypeStruct((GROUP, wide), jnp.bfloat16),
-            jax.ShapeDtypeStruct((dispatch.shape[0], LANES), jnp.bfloat16),
+            jax.ShapeDtypeStruct((dispatch.shape[0] * wide // LANES, LANES), jnp.bfloat16),
         ),
         in_specs=[vector] * 2,
         out_specs=(vector, vector),
@@ -229,52 +244,53 @@
     )(got, dispatch)
 
 
-def expert_kernel(rows, packed, side, out, turned):
-    count, blocks = turned.shape[0], turned.shape[1]
-    wide, hidden = blocks * LANES, packed.shape[1]
-    turned[...] = rows[...].astype(jnp.float32).reshape(turned.shape)
-    features = jnp.concatenate(
-        [turned[:, j, :].astype(jnp.bfloat16) for j in range(blocks)], axis=1
-    )
+def expert_kernel(rows, packed, side, out):
+    hidden = packed.shape[1]
+    wide = packed.shape[0] // 3
+    count = rows.shape[0] * LANES // wide
+    features = rows[...].reshape(count, wide)
 
     def silu_times(weights):
-        gated = jnp.dot(features, weights[0:wide], preferred_element_type=jnp.float32)
-        upped = jnp.dot(features, weights[wide : 2 * wide], preferred_element_type=jnp.float32)
+        joined = jnp.concatenate([weights[0:wide], weights[wide : 2 * wide]], axis=1)
+        product = jnp.dot(features, joined, preferred_element_type=jnp.float32)
+        gated, upped = product[:, :hidden], product[:, hidden:]
         return (gated / (1.0 + jnp.exp(-gated)) * upped).astype(jnp.bfloat16)
 
-    own = silu_times(packed)
-    other = silu_times(side)
-    for j in range(blocks):
-        at = 2 * wide + j * hidden
-        turned[:, j, :] = jnp.dot(
-            own, packed[at : at + hidden], preferred_element_type=jnp.float32
-        ) + jnp.dot(other, side[at : at + hidden], preferred_element_type=jnp.float32)
-    out[...] = turned[...].reshape(out.shape).astype(jnp.bfloat16)
-
-
-def run_expert(rows, packed, side, count):
-    blocks = rows.shape[0] // count
+    both = jnp.concatenate([silu_times(packed), silu_times(side)], axis=1)
+    pieces = []
+    for j in range(0, wide // LANES, 2):
+        at, past = 2 * wide + j * hidden, 2 * wide + (j + 1) * hidden
+        down = jnp.concatenate(
+            [
+                jnp.concatenate([part[at : at + hidden], part[past : past + hidden]], axis=1)
+                for part in (packed, side)
+            ],
+            axis=0,
+        )
+        pieces.append(jnp.dot(both, down, preferred_element_type=jnp.float32).astype(jnp.bfloat16))
+    out[...] = jnp.concatenate(pieces, axis=1).reshape(out.shape)
+
+
+def run_expert(rows, packed, side):
     vector = pl.BlockSpec(memory_space=pltpu.VMEM)
     return pl.pallas_call(
         expert_kernel,
         out_shape=jax.ShapeDtypeStruct(rows.shape, jnp.bfloat16),
         in_specs=[vector] * 3,
         out_specs=vector,
-        scratch_shapes=[pltpu.VMEM((count, blocks, LANES), jnp.float32)],
         compiler_params=GRANT,
         name="expert",
     )(rows, packed, side)
 
 
 def combine_kernel(high, low, returned, shared, out):
-    total = high.shape[0]
-    sums = jnp.dot(high[...], returned[...], preferred_element_type=jnp.float32)
-    sums = sums + jnp.dot(low[...], returned[...], preferred_element_type=jnp.float32)
-    for j in range(total // GROUP):
-        at = slice(j * LANES, (j + 1) * LANES)
-        piece = (sums[j * GROUP : (j + 1) * GROUP] + shared[:, at]).astype(jnp.bfloat16)
-        for d in range(out.shape[0]):
-            out[d, :, at] = piece
+    wide = shared.shape[1]
+    results = returned[...].reshape(returned.shape[0] * LANES // wide, wide)
+    sums = jnp.dot(high[...], results, preferred_element_type=jnp.float32)
+    sums = sums + jnp.dot(low[...], results, preferred_element_type=jnp.float32)
+    sums = (sums + shared[...]).astype(jnp.bfloat16)
+    for d in range(out.shape[0]):
+        out[d] = sums
 
 
 def combine_parts(combine, returned, shared, copies):
@@ -289,7 +305,7 @@
     )(*combine, returned, shared)
 
 
-def finish_kernel(place, partials, whole, gain, bias, out, after):
+def finish_kernel(partials, whole, gain, bias, out, after):
     rows, columns = out.shape
     blocks = []
     for j in range(whole.shape[1] // LANES):
@@ -300,51 +316,41 @@
         after[:, at] = block
         blocks.append(block)
     centre, scale = row_moments(blocks, len(blocks) * LANES)
-    start = pl.multiple_of(place[0] * columns, columns)
+    start = pl.multiple_of(lax.axis_index("tp") * columns, columns)
     own = after[:, pl.ds(start, columns)]
     own = (own - centre) * scale * gain[...] + bias[...]
     out[...] = own[0:rows].astype(jnp.bfloat16)
 
 
-def finish(place, partials, whole, gain, bias, rows):
+def finish(partials, whole, gain, bias, rows):
     vector = pl.BlockSpec(memory_space=pltpu.VMEM)
     return pl.pallas_call(
         finish_kernel,
         out_shape=jax.ShapeDtypeStruct((rows, gain.shape[0]), jnp.bfloat16),
-        in_specs=[pl.BlockSpec(memory_space=pltpu.SMEM)] + [vector] * 4,
+        in_specs=[vector] * 4,
         out_specs=vector,
         scratch_shapes=[pltpu.VMEM(whole.shape, jnp.float32)],
         compiler_params=GRANT,
         name="finish",
-    )(place.reshape(1), partials, whole, gain.reshape(1, -1), bias.reshape(1, -1))
+    )(partials, whole, gain.reshape(1, -1), bias.reshape(1, -1))
 
 
 def exchanged(blocks, axis):
     return lax.all_to_all(blocks, axis, split_axis=0, concat_axis=0, tiled=True)
 
 
-def padded_rows(values, fill):
-    short = GROUP - values.shape[0]
-    return jnp.pad(values, ((0, short), (0, 0)), constant_values=fill)
-
-
-def picks_of(routes, route_weights, mine, experts, blocks):
+def picks_of(routes, route_weights, mine, experts):
     chosen = routes.reshape(-1)
     order = jnp.arange(chosen.shape[0])
     earlier = (chosen[:, None] == chosen[None, :]) & (order[None, :] < order[:, None])
     slots = jnp.sum(earlier.astype(jnp.int32), axis=1).reshape(routes.shape)
-    target = padded_rows(jnp.where(slots == mine, routes, -1), -1)
-    weight = padded_rows(route_weights, 0.0)
-    target = jnp.tile(target, (blocks, 1))
-    weight = jnp.tile(weight, (blocks, 1))
-    shape = (blocks * GROUP, experts * blocks)
-    block = lax.broadcasted_iota(jnp.int32, shape, 0) // GROUP
-    column = lax.broadcasted_iota(jnp.int32, shape, 1)
-    expert = jnp.where(column % blocks == block, column // blocks, -2)
-    picked = jnp.zeros(shape, jnp.float32)
-    combine = jnp.zeros(shape, jnp.float32)
+    short = ((0, GROUP - routes.shape[0]), (0, 0))
+    target = jnp.pad(jnp.where(slots == mine, routes, -1), short, constant_values=-1)
+    weight = jnp.pad(route_weights, short)
+    picked = jnp.zeros((GROUP, experts), jnp.float32)
+    combine = jnp.zeros((GROUP, experts), jnp.float32)
     for k in range(routes.shape[1]):
-        hit = target[:, k : k + 1] == expert
+        hit = target[:, k : k + 1] == jnp.arange(experts)[None, :]
         picked = picked + jnp.where(hit, 1.0, 0.0)
         combine = combine + jnp.where(hit, weight[:, k : k + 1], 0.0)
     high = lax.reduce_precision(combine, 8, 7)
@@ -385,7 +391,7 @@
         expert_gate, expert_up, expert_down, peers,
     )
     reads = exchanged(mixed, "tp").reshape(peers * PADDED, H * HD)
-    dispatch, combine = picks_of(routes, route_weights, place % 2, experts, blocks)
+    dispatch, combine = picks_of(routes, route_weights, place % 2, experts)
     sent = project(reads, out_weight, residual_in, norm1_gain, norm1_bias, peers)
     got = exchanged(sent, "tp")
 
@@ -398,18 +404,19 @@
 
     whole, parcel = normalize_and_pick(got, dispatch, rows)
     arrived = exchanged(parcel.reshape(experts, blocks, LANES), "ep")
-    produced = run_expert(arrived.reshape(experts * blocks, LANES), packed, side, experts)
-    returned = exchanged(produced.reshape(experts, blocks, LANES), "ep")
     shared_hidden = (
         jax.nn.silu(jnp.dot(whole, shared_gate, preferred_element_type=jnp.float32))
         * jnp.dot(whole, shared_up, preferred_element_type=jnp.float32)
     ).astype(jnp.bfloat16)
     shared = jnp.dot(shared_hidden, shared_down, preferred_element_type=jnp.float32)
+    side, shared, combine = lax.optimization_barrier((side, shared, combine))
+    produced = run_expert(arrived.reshape(experts * blocks, LANES), packed, side)
+    returned = exchanged(produced.reshape(experts, blocks, LANES), "ep")
     partial = combine_parts(
         combine, returned.reshape(experts * blocks, LANES), shared, peers
     )
     partials = exchanged(partial, "tp")
-    return finish(place, partials, whole, norm2_gain, norm2_bias, rows)
+    return finish(partials, whole, norm2_gain, norm2_bias, rows)
 
 
 def solution(mesh):
@@ -435,4 +442,5 @@
         P("tp"),
     )
     out_specs = P("ep", "tp")
+
     return jax.shard_map(body, mesh=mesh, in_specs=in_specs, out_specs=out_specs, check_vma=False)

time: 94.1 us -> 91.2 us (0.969)
  blocking collectives: 7.76 us -> 28 us
  waiting for transfers between devices: 32.1 us -> 19.8 us
  starting transfers between devices: 38.9 us -> 33.6 us
  other arithmetic: 3.18 us -> 0.35 us
  Pallas kernels: 10.3 us -> 7.79 us
    all_to_all x1 -> x2, blocking collectives: 7.76 us -> 28 us  [exchanged(): return lax.all_to_all(blocks, axis, split_axis=0, concat_axis=0, tiled=True)]
    all_to_all x4 -> x3, waiting for transfers between devices: 32.1 us -> 19.8 us  [exchanged(): return lax.all_to_all(blocks, axis, split_axis=0, concat_axis=0, tiled=True)]
    all_to_all x4 -> x3, starting transfers between devices: 34.4 us -> 29 us  [exchanged(): return lax.all_to_all(blocks, axis, split_axis=0, concat_axis=0, tiled=True)]
    pallas_call x1, Pallas kernels: 2.1 us -> 0.62 us  [run_expert(): pl.pallas_call(expert_kernel, out_shape=jax.ShapeDtypeStruct(rows.shape,...]
    convert_element_type x2 -> x1, other arithmetic: 1.54 us -> 0.11 us  [picks_of(): parts = (high.astype(jnp.bfloat16), (combine - high).astype(jnp.bfloat16))]
    convert_element_type x1, other arithmetic: 1.41 us -> 0.05 us  [picks_of(): return (picked.T.astype(jnp.bfloat16), parts)]
  transfers between devices with their start and end apart: 5 -> 4, of which waited for: 3 -> 2; matrix products, arithmetic and copies ran while one was open for 4% -> 1% of each run, Pallas kernels for 2% -> 2%
where the time goes in v4:
time: 91.2 us; the launch traced here: 90.8 us
  starting transfers between devices  33.6 us (37%)
  blocking collectives  28 us (31%)
  waiting for transfers between devices  19.8 us (22%)
  Pallas kernels  7.79 us (9%)
    all_to_all x3, starting transfers between devices, exchanged(): return lax.all_to_all(blocks, axis, split_axis=0, concat_axis=0, tiled=True)  29 us
    all_to_all x2, blocking collectives, exchanged(): return lax.all_to_all(blocks, axis, split_axis=0, concat_axis=0, tiled=True)  28 us
    all_to_all x3, waiting for transfers between devices, exchanged(): return lax.all_to_all(blocks, axis, split_axis=0, concat_axis=0, tiled=True)  19.8 us
    ppermute x1, starting transfers between devices, body(): side = lax.ppermute(packed, ('ep', 'tp'), swaps)  4.57 us
    pallas_call x1, Pallas kernels, stick_read(): pl.pallas_call(stick_kernel, out_shape=(jax.ShapeDtypeStruct((copies, PAD...  4.3 us
  transfers between devices with their start and end apart: 4, of which 2 were waited for; matrix products, arithmetic and copies ran while one was open for 1% of the time, Pallas kernels for 2%

profile of v4, /device:TPU:1, one launch (start us, length us, event | category | flops | bytes accessed | tf_op | source)
XLA Modules:
  0.0 90.8 jit_solution(3079134072607746342)
XLA Ops:
  0.0 0.0 copy-start
  0.0 0.0 copy-start.10
  0.0 0.0 copy-start.4
  0.0 0.0 copy-start.3
  0.0 0.0 copy-start.1
  0.0 0.0 copy-start.2
  0.0 0.0 copy-start.9
  0.1 4.3 %stick.1 = (bf16[4,8,512]{2,1,0:T(8,128)(2,1)}, bf16[3072,128]{1,0:T(8,128)(2,1)S(1)}) custom-call(s32[5]{0:T(128)} %lengths_at.1, f32[8]{0:T(128)} %offsets_at.1, bf16[5,512]{1,0:T(8,128)(2,1)} %queries_at.1, bf16[5,1024,128]{2,1,0:T(8,128)(2,1)} %keys.1, bf16[5,1024,128]{2,1,0:T(8,128)(2,1)} %values.1, bf16[1,1024,128]{2,1,0:T(8,128)(2,1)} %gate.1, ...), custom_call_target="tpu_custom_call" | custom-call | tf_op jit(solution)/shard_map/stick/pallas_call | solution.py:137
  4.4 0.0 copy-start.7
  4.4 0.0 copy-start.8
  4.4 5.0 %all-to-all-start = ((bf16[4,8,512]{2,1,0:T(8,128)(2,1)}), bf16[4,8,512]{2,1,0:T(8,128)(2,1)S(1)}, u32[]{:S(2)}, u32[]{:S(2)}) async-start(bf16[4,8,512]{2,1,0:T(8,128)(2,1)} %get-tuple-element.14), calls=%async_computation | async-start | bytes 65536 | tf_op jit(solution)/shard_map/all_to_all | solution.py:339
  9.4 4.6 %collective-permute-start = (bf16[3072,128]{1,0:T(8,128)(2,1)S(1)}, bf16[3072,128]{1,0:T(8,128)(2,1)S(1)}, u32[]{:S(2)}, u32[]{:S(2)}) collective-permute-start(bf16[3072,128]{1,0:T(8,128)(2,1)S(1)} %get-tuple-element.13.packed), channel_id=1, source_target_pairs={{0,1},{1,0},{2,3},{3,2},{4,7},{5,6},{6,5},{7,4},{8,9},{9,8},{10,11... | collective-permute-start | bytes 2359304 | tf_op jit(solution)/shard_map/ppermute | solution.py:403
  13.9 0.0 copy-done.10
  14.0 0.1 copy.24
  14.1 0.1 eq.158
  14.1 0.2 convert_reduce_fusion
  14.3 0.1 eq.164
  14.5 0.3 slice_reduce_fusion.5
  14.7 0.1 add_convert_fusion.dispatch
  14.8 0.0 all-to-all-done
  14.8 0.0 copy-done.4
  14.8 0.0 copy-done.3
  14.8 0.0 copy-done.1
  14.8 0.0 copy-done.2
  14.8 0.8 project.1
  15.6 3.3 %all-to-all-start.1 = ((f32[4,24,256]{2,1,0:T(8,128)}), f32[4,24,256]{2,1,0:T(8,128)S(1)}, u32[]{:S(2)}, u32[]{:S(2)}) async-start(f32[4,24,256]{2,1,0:T(8,128)} %project.1), calls=%async_computation.1 | async-start | bytes 196608 | tf_op jit(solution)/shard_map/all_to_all | solution.py:339
  18.9 0.0 copy-done.9
  19.0 5.1 %all-to-all-done.1.got = f32[4,24,256]{2,1,0:T(8,128)S(1)} async-done(((f32[4,24,256]{2,1,0:T(8,128)}), f32[4,24,256]{2,1,0:T(8,128)S(1)}, u32[]{:S(2)}, u32[]{:S(2)}) %all-to-all-start.1) | async-done | bytes 98336 | tf_op jit(solution)/shard_map/all_to_all | solution.py:339
  24.1 1.1 %norm.1 = (bf16[24,1024]{1,0:T(8,128)(2,1)S(1)}, bf16[1024,128]{1,0:T(8,128)(2,1)}) custom-call(f32[4,24,256]{2,1,0:T(8,128)S(1)} %all-to-all-done.1.got, bf16[128,24]{1,0:T(8,128)(2,1)S(1)} %add_convert_fusion.dispatch), custom_call_target="tpu_custom_call" | custom-call | tf_op jit(solution)/shard_map/norm/pallas_call | solution.py:234
  25.2 20.7 %all-to-all-start.2 = ((bf16[128,8,128]{2,1,0:T(8,128)(2,1)}), bf16[128,8,128]{2,1,0:T(8,128)(2,1)S(1)}, u32[]{:S(2)}, u32[]{:S(2)}) async-start(bf16[128,8,128]{2,1,0:T(8,128)(2,1)} %bitcast.9), calls=%async_computation.2 | async-start | bytes 524288 | tf_op jit(solution)/shard_map/all_to_all | solution.py:339
  45.9 0.1 fusion.3
  46.0 0.0 copy-done.7
  46.0 0.2 fusion.17
  46.2 0.0 copy-done
  46.2 0.0 copy-done.8
  46.2 0.3 fusion.1.shared
  46.5 0.0 collective-permute-done.side
  46.5 14.6 %all-to-all-done.2 = bf16[128,8,128]{2,1,0:T(8,128)(2,1)S(1)} async-done(((bf16[128,8,128]{2,1,0:T(8,128)(2,1)}), bf16[128,8,128]{2,1,0:T(8,128)(2,1)S(1)}, u32[]{:S(2)}, u32[]{:S(2)}) %all-to-all-start.2) | async-done | bytes 262176 | tf_op jit(solution)/shard_map/all_to_all | solution.py:339
  61.1 0.0 copy-start.5
  61.2 0.0 copy-start.6
  61.2 0.6 expert.1
  61.8 20.2 %all_to_all.25 = bf16[128,8,128]{2,1,0:T(8,128)(2,1)S(1)} all-to-all(bf16[128,8,128]{2,1,0:T(8,128)(2,1)S(1)} %bitcast.28), channel_id=1, replica_groups=mesh['ep'=128,'tp'=4] {'ep'}, dimensions={0} | all-to-all | bytes 524288 | tf_op jit(solution)/shard_map/all_to_all | solution.py:339
  82.0 0.3 combine.1
  82.3 7.8 %all_to_all.26.partials = bf16[4,24,1024]{2,1,0:T(8,128)(2,1)S(1)} all-to-all(bf16[4,24,1024]{2,1,0:T(8,128)(2,1)S(1)} %combine.1), channel_id=1, replica_groups=mesh['ep'=128,'tp'=4] {'tp'}, dimensions={0} | all-to-all | bytes 393216 | tf_op jit(solution)/shard_map/all_to_all | solution.py:339
  90.0 0.0 copy-done.5
  90.0 0.0 copy-done.6
  90.0 0.7 finish.1
  (3 shorter events, 0.0 us)
Async XLA Ops:
  0.0 46.2 %copy-start = (bf16[128,1024]{1,0:T(8,128)(2,1)S(1)}, bf16[128,1024]{1,0:T(8,128)(2,1)}, u32[]{:S(2)}) copy-start(bf16[128,1024]{1,0:T(8,128)(2,1)} %param.35) | copy-start | bytes 786436
  0.0 13.9 %copy-start.10 = (s32[20,6]{0,1:T(8,128)S(1)}, s32[20,6]{0,1:T(8,128)}, u32[]{:S(2)}) copy-start(s32[20,6]{0,1:T(8,128)} %param.28) | copy-start | bytes 1444
  0.0 14.8 %copy-start.4 = (f32[256]{0:T(256)S(1)}, f32[256]{0:T(256)}, u32[]{:S(2)}) copy-start(f32[256]{0:T(256)} %param.27) | copy-start | bytes 3076
  0.0 14.8 %copy-start.3 = (f32[256]{0:T(256)S(1)}, f32[256]{0:T(256)}, u32[]{:S(2)}) copy-start(f32[256]{0:T(256)} %param.26) | copy-start | bytes 3076
  0.0 14.8 %copy-start.1 = (bf16[512,256]{1,0:T(8,128)(2,1)S(1)}, bf16[512,256]{1,0:T(8,128)(2,1)}, u32[]{:S(2)}) copy-start(bf16[512,256]{1,0:T(8,128)(2,1)} %weight.1) | copy-start | bytes 786436
  0.0 14.8 %copy-start.2 = (bf16[20,256]{1,0:T(8,128)(2,1)S(1)}, bf16[20,256]{1,0:T(8,128)(2,1)}, u32[]{:S(2)}) copy-start(bf16[20,256]{1,0:T(8,128)(2,1)} %residual.1) | copy-start | bytes 30724
  0.0 18.9 %copy-start.9 = (f32[20,6]{0,1:T(8,128)S(1)}, f32[20,6]{0,1:T(8,128)}, u32[]{:S(2)}) copy-start(f32[20,6]{0,1:T(8,128)} %param.29) | copy-start | bytes 1444
  4.4 41.7 %copy-start.7 = (bf16[1024,128]{1,0:T(8,128)(2,1)S(1)}, bf16[1024,128]{1,0:T(8,128)(2,1)}, u32[]{:S(2)}) copy-start(bf16[1024,128]{1,0:T(8,128)(2,1)} %param.33) | copy-start | bytes 786436
  4.4 41.8 %copy-start.8 = (bf16[1024,128]{1,0:T(8,128)(2,1)S(1)}, bf16[1024,128]{1,0:T(8,128)(2,1)}, u32[]{:S(2)}) copy-start(bf16[1024,128]{1,0:T(8,128)(2,1)} %param.34) | copy-start | bytes 786436
  4.4 10.4 %all-to-all-start = ((bf16[4,8,512]{2,1,0:T(8,128)(2,1)}), bf16[4,8,512]{2,1,0:T(8,128)(2,1)S(1)}, u32[]{:S(2)}, u32[]{:S(2)}) async-start(bf16[4,8,512]{2,1,0:T(8,128)(2,1)} %get-tuple-element.14), calls=%async_computation | async-start | bytes 65536 | tf_op jit(solution)/shard_map/all_to_all | solution.py:339
  9.4 37.1 %collective-permute-start = (bf16[3072,128]{1,0:T(8,128)(2,1)S(1)}, bf16[3072,128]{1,0:T(8,128)(2,1)S(1)}, u32[]{:S(2)}, u32[]{:S(2)}) collective-permute-start(bf16[3072,128]{1,0:T(8,128)(2,1)S(1)} %get-tuple-element.13.packed), channel_id=1, source_target_pairs={{0,1},{1,0},{2,3},{3,2},{4,7},{5,6},{6,5},{7,4},{8,9},{9,8},{10,11... | collective-permute-start | bytes 2359304 | tf_op jit(solution)/shard_map/ppermute | solution.py:403
  15.6 8.4 %all-to-all-start.1 = ((f32[4,24,256]{2,1,0:T(8,128)}), f32[4,24,256]{2,1,0:T(8,128)S(1)}, u32[]{:S(2)}, u32[]{:S(2)}) async-start(f32[4,24,256]{2,1,0:T(8,128)} %project.1), calls=%async_computation.1 | async-start | bytes 196608 | tf_op jit(solution)/shard_map/all_to_all | solution.py:339
  25.2 36.0 %all-to-all-start.2 = ((bf16[128,8,128]{2,1,0:T(8,128)(2,1)}), bf16[128,8,128]{2,1,0:T(8,128)(2,1)S(1)}, u32[]{:S(2)}, u32[]{:S(2)}) async-start(bf16[128,8,128]{2,1,0:T(8,128)(2,1)} %bitcast.9), calls=%async_computation.2 | async-start | bytes 524288 | tf_op jit(solution)/shard_map/all_to_all | solution.py:339
  61.1 28.9 %copy-start.5 = (f32[256]{0:T(256)S(1)}, f32[256]{0:T(256)}, u32[]{:S(2)}) copy-start(f32[256]{0:T(256)} %param.36) | copy-start | bytes 3076
  61.2 28.9 %copy-start.6 = (f32[256]{0:T(256)S(1)}, f32[256]{0:T(256)}, u32[]{:S(2)}) copy-start(f32[256]{0:T(256)} %param.37) | copy-start | bytes 3076

commit v5 on v4

--- a/solution.py
+++ b/solution.py
@@ -22,9 +22,38 @@
 EPSILON = 1e-05
 
 
+def route_tables(routes, shares, chosen, share, dispatch, high, low):
+    picks, tokens = routes.shape
+    chosen[...] = jnp.full(chosen.shape, -1, jnp.int32)
+    share[...] = jnp.zeros(share.shape, jnp.float32)
+    chosen[0:picks, 0:tokens] = routes[...]
+    share[0:picks, 0:tokens] = shares[...]
+    shape = (dispatch.shape[0], LANES)
+    expert = lax.broadcasted_iota(jnp.int32, shape, 0)
+    hits = [chosen[k : k + 1, :] == expert for k in range(picks)]
+    named = jnp.zeros(shape, jnp.float32)
+    for hit in hits:
+        named = jnp.where(hit, 1.0, named)
+    before = lax.broadcasted_iota(jnp.int32, (LANES, LANES), 0)
+    token = lax.broadcasted_iota(jnp.int32, (LANES, LANES), 1)
+    sooner = jnp.where(before < token, 1.0, 0.0).astype(jnp.bfloat16)
+    slot = jnp.dot(named.astype(jnp.bfloat16), sooner, preferred_element_type=jnp.float32)
+    mine = (lax.axis_index("tp") % 2).astype(jnp.float32)
+    held = slot == mine
+    dispatch[...] = jnp.where(held, named, 0.0).astype(jnp.bfloat16)
+    weight = jnp.zeros(shape, jnp.float32)
+    for k, hit in enumerate(hits):
+        weight = jnp.where(hit & held, share[k : k + 1, :], weight)
+    weight = weight.T[0 : high.shape[0]]
+    upper = weight.astype(jnp.bfloat16)
+    high[...] = upper
+    low[...] = (weight - upper.astype(jnp.float32)).astype(jnp.bfloat16)
+
+
 def stick_kernel(
-    lengths_at, offsets_at, queries_at, keys, values, gate, up, down,
-    out, packed, lengths, offsets, queries, keys_vm, values_vm, reads,
+    lengths_at, offsets_at, queries_at, routes_at, shares_at, keys, values, gate, up, down,
+    out, packed, dispatch, high, low,
+    lengths, offsets, queries, routes, shares, chosen, share, keys_vm, values_vm, reads,
     small_sems, key_sems, value_sems, pack_sems,
 ):
     seqs = keys.shape[0]
@@ -47,13 +76,20 @@
     small_copies = [
         pltpu.make_async_copy(source, target, small_sems.at[i])
         for i, (source, target) in enumerate(
-            ((queries_at, queries), (lengths_at, lengths), (offsets_at, offsets))
+            (
+                (routes_at, routes),
+                (shares_at, shares),
+                (queries_at, queries),
+                (lengths_at, lengths),
+                (offsets_at, offsets),
+            )
         )
     ]
     for copy in small_copies + key_copies + value_copies + pack_copies:
         copy.start()
     for copy in small_copies:
         copy.wait()
+    route_tables(routes, shares, chosen, share, dispatch, high, low)
 
     row = lax.broadcasted_iota(jnp.int32, (H, LANES), 0)
     lane = lax.broadcasted_iota(jnp.int32, (H, LANES), 1)
@@ -129,7 +165,9 @@
         copy.wait()
 
 
-def stick_read(queries, keys, values, lengths, offsets, gate, up, down, copies):
+def stick_read(
+    queries, keys, values, lengths, offsets, routes, shares, gate, up, down, copies, experts
+):
     seqs = queries.shape[0]
     wide, hidden = gate.shape[1], gate.shape[2]
     anywhere = pl.BlockSpec(memory_space=pltpu.HBM)
@@ -139,17 +177,24 @@
         out_shape=(
             jax.ShapeDtypeStruct((copies, PADDED, H * HD), jnp.bfloat16),
             jax.ShapeDtypeStruct((3 * wide, hidden), jnp.bfloat16),
+            jax.ShapeDtypeStruct((experts, LANES), jnp.bfloat16),
+            jax.ShapeDtypeStruct((GROUP, experts), jnp.bfloat16),
+            jax.ShapeDtypeStruct((GROUP, experts), jnp.bfloat16),
         ),
-        in_specs=[anywhere] * 8,
-        out_specs=(vector, vector),
+        in_specs=[anywhere] * 10,
+        out_specs=(vector,) * 5,
         scratch_shapes=[
             pltpu.SMEM(lengths.shape, jnp.int32),
             pltpu.SMEM(offsets.shape, jnp.float32),
             pltpu.VMEM(queries.shape, jnp.bfloat16),
+            pltpu.VMEM(routes.shape, jnp.int32),
+            pltpu.VMEM(shares.shape, jnp.float32),
+            pltpu.VMEM((8, LANES), jnp.int32),
+            pltpu.VMEM((8, LANES), jnp.float32),
             pltpu.VMEM(keys.shape, jnp.bfloat16),
             pltpu.VMEM(values.shape, jnp.bfloat16),
             pltpu.VMEM((PADDED, H * HD), jnp.float32),
-            pltpu.SemaphoreType.DMA((3,)),
+            pltpu.SemaphoreType.DMA((5,)),
             pltpu.SemaphoreType.DMA((seqs,)),
             pltpu.SemaphoreType.DMA((seqs,)),
             pltpu.SemaphoreType.DMA((2 + wide // LANES,)),
@@ -158,7 +203,7 @@
         name="stick",
     )(*(
         pltpu.with_memory_space_constraint(x, pltpu.HBM)
-        for x in (lengths, offsets, queries, keys, values, gate, up, down)
+        for x in (lengths, offsets, queries, routes, shares, keys, values, gate, up, down)
     ))
 
 
@@ -224,7 +269,7 @@
     ]
     normed = jnp.concatenate(normed, axis=1).astype(jnp.bfloat16)
     whole[...] = normed
-    picked = jnp.dot(dispatch[...], normed, preferred_element_type=jnp.float32)
+    picked = jnp.dot(dispatch[:, 0:GROUP], normed, preferred_element_type=jnp.float32)
     parcel[...] = picked.astype(jnp.bfloat16).reshape(parcel.shape)
 
 
@@ -337,25 +382,6 @@
 
 def exchanged(blocks, axis):
     return lax.all_to_all(blocks, axis, split_axis=0, concat_axis=0, tiled=True)
-
-
-def picks_of(routes, route_weights, mine, experts):
-    chosen = routes.reshape(-1)
-    order = jnp.arange(chosen.shape[0])
-    earlier = (chosen[:, None] == chosen[None, :]) & (order[None, :] < order[:, None])
-    slots = jnp.sum(earlier.astype(jnp.int32), axis=1).reshape(routes.shape)
-    short = ((0, GROUP - routes.shape[0]), (0, 0))
-    target = jnp.pad(jnp.where(slots == mine, routes, -1), short, constant_values=-1)
-    weight = jnp.pad(route_weights, short)
-    picked = jnp.zeros((GROUP, experts), jnp.float32)
-    combine = jnp.zeros((GROUP, experts), jnp.float32)
-    for k in range(routes.shape[1]):
-        hit = target[:, k : k + 1] == jnp.arange(experts)[None, :]
-        picked = picked + jnp.where(hit, 1.0, 0.0)
-        combine = combine + jnp.where(hit, weight[:, k : k + 1], 0.0)
-    high = lax.reduce_precision(combine, 8, 7)
-    parts = (high.astype(jnp.bfloat16), (combine - high).astype(jnp.bfloat16))
-    return picked.T.astype(jnp.bfloat16), parts
 
 
 def body(
@@ -381,17 +407,15 @@
 ):
     peers = lax.axis_size("tp")
     experts = lax.axis_size("ep")
-    place = lax.axis_index("tp")
     rows, columns = residual_in.shape
     wide = columns * peers
     blocks = wide // LANES
 
-    mixed, packed = stick_read(
-        queries, cache_keys, cache_values, lengths, stick_offset,
-        expert_gate, expert_up, expert_down, peers,
+    mixed, packed, dispatch, high, low = stick_read(
+        queries, cache_keys, cache_values, lengths, stick_offset, routes.T, route_weights.T,
+        expert_gate, expert_up, expert_down, peers, experts,
     )
     reads = exchanged(mixed, "tp").reshape(peers * PADDED, H * HD)
-    dispatch, combine = picks_of(routes, route_weights, place % 2, experts)
     sent = project(reads, out_weight, residual_in, norm1_gain, norm1_bias, peers)
     got = exchanged(sent, "tp")
 
@@ -409,11 +433,11 @@
         * jnp.dot(whole, shared_up, preferred_element_type=jnp.float32)
     ).astype(jnp.bfloat16)
     shared = jnp.dot(shared_hidden, shared_down, preferred_element_type=jnp.float32)
-    side, shared, combine = lax.optimization_barrier((side, shared, combine))
+    side, shared = lax.optimization_barrier((side, shared))
     produced = run_expert(arrived.reshape(experts * blocks, LANES), packed, side)
     returned = exchanged(produced.reshape(experts, blocks, LANES), "ep")
     partial = combine_parts(
-        combine, returned.reshape(experts * blocks, LANES), shared, peers
+        (high, low), returned.reshape(experts * blocks, LANES), shared, peers
     )
     partials = exchanged(partial, "tp")
     return finish(partials, whole, norm2_gain, norm2_bias, rows)

time: 91.2 us -> 93.6 us (1.026)
  blocking collectives: 28 us -> 46 us
  starting transfers between devices: 33.6 us -> 25.1 us
  waiting for transfers between devices: 19.8 us -> 14.8 us
  Pallas kernels: 7.79 us -> 6.75 us
    all_to_all x2 -> x4, blocking collectives: 28 us -> 46 us  [exchanged(): return lax.all_to_all(blocks, axis, split_axis=0, concat_axis=0, tiled=True)]
    all_to_all x3 -> x1, starting transfers between devices: 29 us -> 19.8 us  [exchanged(): return lax.all_to_all(blocks, axis, split_axis=0, concat_axis=0, tiled=True)]
    all_to_all x3 -> x1, waiting for transfers between devices: 19.8 us -> 14.8 us  [exchanged(): return lax.all_to_all(blocks, axis, split_axis=0, concat_axis=0, tiled=True)]
  transfers between devices with their start and end apart: 4 -> 2, of which waited for: 2 -> 1; matrix products, arithmetic and copies ran while one was open for 1% -> 0% of each run, Pallas kernels for 2% -> 1%
where the time goes in v5:
time: 93.6 us; the launch traced here: 93.2 us
  blocking collectives  46 us (49%)
  starting transfers between devices  25.1 us (27%)
  waiting for transfers between devices  14.8 us (16%)
  Pallas kernels  6.75 us (7%)
    all_to_all x4, blocking collectives, exchanged(): return lax.all_to_all(blocks, axis, split_axis=0, concat_axis=0, tiled=True)  46 us
    all_to_all x1, starting transfers between devices, exchanged(): return lax.all_to_all(blocks, axis, split_axis=0, concat_axis=0, tiled=True)  19.8 us
    all_to_all x1, waiting for transfers between devices, exchanged(): return lax.all_to_all(blocks, axis, split_axis=0, concat_axis=0, tiled=True)  14.8 us
    ppermute x1, starting transfers between devices, body(): side = lax.ppermute(packed, ('ep', 'tp'), swaps)  5.34 us
    pallas_call x1, Pallas kernels, stick_read(): pl.pallas_call(stick_kernel, out_shape=(jax.ShapeDtypeStruct((copies, PAD...  3.89 us
  transfers between devices with their start and end apart: 2, of which 1 were waited for; matrix products, arithmetic and copies ran while one was open for 0% of the time, Pallas kernels for 1%

profile of v5, /device:TPU:1, one launch (start us, length us, event | category | flops | bytes accessed | tf_op | source)
XLA Modules:
  0.0 93.2 jit_solution(12831282897908457203)
XLA Ops:
  0.0 0.0 copy-start
  0.0 0.0 copy-start.1
  0.0 0.0 copy-start.2
  0.0 0.0 copy-start.3
  0.0 0.0 copy-start.4
  0.0 3.9 %stick.1 = (bf16[4,8,512]{2,1,0:T(8,128)(2,1)S(1)}, bf16[3072,128]{1,0:T(8,128)(2,1)S(1)}, bf16[128,128]{1,0:T(8,128)(2,1)S(1)}, bf16[24,128]{1,0:T(8,128)(2,1)S(1)}, bf16[24,128]{1,0:T(8,128)(2,1)S(1)}) custom-call(s32[5]{0:T(128)} %lengths_at.1, f32[8]{0:T(128)} %offsets_at.1, bf16[5,512]{1,0:T(8,128)(2,1)} %queries_at.1, s32[6,20]{1,0:T(8,128)} %bitcast.24, ...), custom_call_target="tpu_custom_call" | custom-call | tf_op jit(solution)/shard_map/stick/pallas_call | solution.py:175
  3.9 0.0 copy-start.7
  3.9 0.0 copy-start.8
  4.0 5.3 %collective-permute-start = (bf16[3072,128]{1,0:T(8,128)(2,1)S(1)}, bf16[3072,128]{1,0:T(8,128)(2,1)S(1)}, u32[]{:S(2)}, u32[]{:S(2)}) collective-permute-start(bf16[3072,128]{1,0:T(8,128)(2,1)S(1)} %get-tuple-element.19.packed), channel_id=1, source_target_pairs={{0,1},{1,0},{2,3},{3,2},{4,7},{5,6},{6,5},{7,4},{8,9},{9,8},{10,11... | collective-permute-start | bytes 2359304 | tf_op jit(solution)/shard_map/ppermute | solution.py:427
  9.3 9.5 %all_to_all.25 = bf16[4,8,512]{2,1,0:T(8,128)(2,1)S(1)} all-to-all(bf16[4,8,512]{2,1,0:T(8,128)(2,1)S(1)} %get-tuple-element.16), channel_id=1, replica_groups=mesh['ep'=128,'tp'=4] {'tp'}, dimensions={0} | all-to-all | bytes 65536 | tf_op jit(solution)/shard_map/all_to_all | solution.py:384
  18.8 0.0 copy-done.1
  18.8 0.0 copy-done.2
  18.8 0.0 copy-done.3
  18.8 0.0 copy-done.4
  18.9 0.2 project.1
  19.0 8.5 %all_to_all.26.got = f32[4,24,256]{2,1,0:T(8,128)S(1)} all-to-all(f32[4,24,256]{2,1,0:T(8,128)S(1)} %project.1), channel_id=1, replica_groups=mesh['ep'=128,'tp'=4] {'tp'}, dimensions={0} | all-to-all | bytes 196608 | tf_op jit(solution)/shard_map/all_to_all | solution.py:384
  27.5 1.1 %norm.1 = (bf16[24,1024]{1,0:T(8,128)(2,1)S(1)}, bf16[1024,128]{1,0:T(8,128)(2,1)}) custom-call(f32[4,24,256]{2,1,0:T(8,128)S(1)} %all_to_all.26.got, bf16[128,128]{1,0:T(8,128)(2,1)S(1)} %get-tuple-element.17.dispatch), custom_call_target="tpu_custom_call" | custom-call | tf_op jit(solution)/shard_map/norm/pallas_call | solution.py:279
  28.6 19.8 %all-to-all-start.2 = ((bf16[128,8,128]{2,1,0:T(8,128)(2,1)}), bf16[128,8,128]{2,1,0:T(8,128)(2,1)S(1)}, u32[]{:S(2)}, u32[]{:S(2)}) async-start(bf16[128,8,128]{2,1,0:T(8,128)(2,1)} %bitcast.5), calls=%async_computation.2 | async-start | bytes 524288 | tf_op jit(solution)/shard_map/all_to_all | solution.py:384
  48.4 0.0 copy-done.7
  48.4 0.2 fusion.9
  48.6 0.0 copy-done
  48.6 0.0 copy-done.8
  48.6 0.3 fusion.1.shared
  48.9 0.0 collective-permute-done.side
  48.9 14.8 %all-to-all-done.2 = bf16[128,8,128]{2,1,0:T(8,128)(2,1)S(1)} async-done(((bf16[128,8,128]{2,1,0:T(8,128)(2,1)}), bf16[128,8,128]{2,1,0:T(8,128)(2,1)S(1)}, u32[]{:S(2)}, u32[]{:S(2)}) %all-to-all-start.2) | async-done | bytes 262176 | tf_op jit(solution)/shard_map/all_to_all | solution.py:384
  63.6 0.0 copy-start.5
  63.6 0.0 copy-start.6
  63.6 0.6 expert.1
  64.2 20.2 %all_to_all.27 = bf16[128,8,128]{2,1,0:T(8,128)(2,1)S(1)} all-to-all(bf16[128,8,128]{2,1,0:T(8,128)(2,1)S(1)} %bitcast.18), channel_id=1, replica_groups=mesh['ep'=128,'tp'=4] {'ep'}, dimensions={0} | all-to-all | bytes 524288 | tf_op jit(solution)/shard_map/all_to_all | solution.py:384
  84.5 0.3 combine.1
  84.7 7.8 %all_to_all.28.partials = bf16[4,24,1024]{2,1,0:T(8,128)(2,1)S(1)} all-to-all(bf16[4,24,1024]{2,1,0:T(8,128)(2,1)S(1)} %combine.1), channel_id=1, replica_groups=mesh['ep'=128,'tp'=4] {'tp'}, dimensions={0} | all-to-all | bytes 393216 | tf_op jit(solution)/shard_map/all_to_all | solution.py:384
  92.5 0.0 copy-done.5
  92.5 0.0 copy-done.6
  92.5 0.7 finish.1
Async XLA Ops:
  0.0 48.6 %copy-start = (bf16[128,1024]{1,0:T(8,128)(2,1)S(1)}, bf16[128,1024]{1,0:T(8,128)(2,1)}, u32[]{:S(2)}) copy-start(bf16[128,1024]{1,0:T(8,128)(2,1)} %param.35) | copy-start | bytes 786436
  0.0 18.8 %copy-start.1 = (bf16[512,256]{1,0:T(8,128)(2,1)S(1)}, bf16[512,256]{1,0:T(8,128)(2,1)}, u32[]{:S(2)}) copy-start(bf16[512,256]{1,0:T(8,128)(2,1)} %weight.1) | copy-start | bytes 786436
  0.0 18.8 %copy-start.2 = (bf16[20,256]{1,0:T(8,128)(2,1)S(1)}, bf16[20,256]{1,0:T(8,128)(2,1)}, u32[]{:S(2)}) copy-start(bf16[20,256]{1,0:T(8,128)(2,1)} %residual.1) | copy-start | bytes 30724
  0.0 18.8 %copy-start.3 = (f32[256]{0:T(256)S(1)}, f32[256]{0:T(256)}, u32[]{:S(2)}) copy-start(f32[256]{0:T(256)} %param.26) | copy-start | bytes 3076
  0.0 18.8 %copy-start.4 = (f32[256]{0:T(256)S(1)}, f32[256]{0:T(256)}, u32[]{:S(2)}) copy-start(f32[256]{0:T(256)} %param.27) | copy-start | bytes 3076
  3.9 44.5 %copy-start.7 = (bf16[1024,128]{1,0:T(8,128)(2,1)S(1)}, bf16[1024,128]{1,0:T(8,128)(2,1)}, u32[]{:S(2)}) copy-start(bf16[1024,128]{1,0:T(8,128)(2,1)} %param.33) | copy-start | bytes 786436
  3.9 44.6 %copy-start.8 = (bf16[1024,128]{1,0:T(8,128)(2,1)S(1)}, bf16[1024,128]{1,0:T(8,128)(2,1)}, u32[]{:S(2)}) copy-start(bf16[1024,128]{1,0:T(8,128)(2,1)} %param.34) | copy-start | bytes 786436
  4.0 44.9 %collective-permute-start = (bf16[3072,128]{1,0:T(8,128)(2,1)S(1)}, bf16[3072,128]{1,0:T(8,128)(2,1)S(1)}, u32[]{:S(2)}, u32[]{:S(2)}) collective-permute-start(bf16[3072,128]{1,0:T(8,128)(2,1)S(1)} %get-tuple-element.19.packed), channel_id=1, source_target_pairs={{0,1},{1,0},{2,3},{3,2},{4,7},{5,6},{6,5},{7,4},{8,9},{9,8},{10,11... | collective-permute-start | bytes 2359304 | tf_op jit(solution)/shard_map/ppermute | solution.py:427
  28.6 35.0 %all-to-all-start.2 = ((bf16[128,8,128]{2,1,0:T(8,128)(2,1)}), bf16[128,8,128]{2,1,0:T(8,128)(2,1)S(1)}, u32[]{:S(2)}, u32[]{:S(2)}) async-start(bf16[128,8,128]{2,1,0:T(8,128)(2,1)} %bitcast.5), calls=%async_computation.2 | async-start | bytes 524288 | tf_op jit(solution)/shard_map/all_to_all | solution.py:384
  63.6 28.9 %copy-start.5 = (f32[256]{0:T(256)S(1)}, f32[256]{0:T(256)}, u32[]{:S(2)}) copy-start(f32[256]{0:T(256)} %param.36) | copy-start | bytes 3076
  63.6 28.9 %copy-start.6 = (f32[256]{0:T(256)S(1)}, f32[256]{0:T(256)}, u32[]{:S(2)}) copy-start(f32[256]{0:T(256)} %param.37) | copy-start | bytes 3076

commit v6 on v5

--- a/solution.py
+++ b/solution.py
@@ -85,7 +85,7 @@
             )
         )
     ]
-    for copy in small_copies + key_copies + value_copies + pack_copies:
+    for copy in small_copies + key_copies + value_copies:
         copy.start()
     for copy in small_copies:
         copy.wait()
@@ -103,7 +103,7 @@
     column = lax.broadcasted_iota(jnp.int32, (LANES, 2 * LANES), 1)
     later = jnp.where((place > column) | (column >= LANES), 1.0, 0.0).astype(jnp.bfloat16)
 
-    stays, takes = [], []
+    built = []
     for s in range(seqs):
         query = jnp.zeros((H, LANES), jnp.float32)
         for h in range(H):
@@ -113,10 +113,20 @@
                 both = pltpu.roll(both, HD, 1)
             query = jnp.where(row == h, both, query)
         query = jnp.where(first == low, query, 0.0).astype(jnp.bfloat16)
-        key_copies[s].wait()
-        scores = lax.dot_general(
-            query, keys_vm[s], (((1,), (1,)), ((), ())), preferred_element_type=jnp.float32
-        )
+        built.append(query)
+    stays, takes = [], []
+    for s in range(seqs):
+        if s % 2 == 0:
+            pair = range(s, min(s + 2, seqs))
+            for p in pair:
+                key_copies[p].wait()
+            joined = jnp.concatenate([built[p] for p in pair], axis=0)
+            keyed = jnp.concatenate([keys_vm[p] for p in pair], axis=0)
+            product = lax.dot_general(
+                joined, keyed, (((1,), (1,)), ((), ())), preferred_element_type=jnp.float32
+            )
+        i = s % 2
+        scores = product[i * H : (i + 1) * H, i * CACHE : (i + 1) * CACHE]
         stay, take = [], []
         for b in range(BLOCKS):
             score = scores[:, b * LANES : (b + 1) * LANES] * HD ** (-0.5) - offset
@@ -127,6 +137,8 @@
         stays.append(stay)
         takes.append(take)
 
+    for copy in pack_copies:
+        copy.start()
     rest = jnp.concatenate([stays[s][b] for b in range(BLOCKS) for s in range(seqs)], axis=0)
     sums = jnp.zeros((BLOCKS * seqs * H, 2 * LANES), jnp.float32)
     for _ in range(3):
@@ -257,7 +269,7 @@
     return centre, lax.rsqrt(spread + EPSILON)
 
 
-def norm_kernel(rows, got, dispatch, whole, parcel):
+def norm_kernel(rows, got, dispatch, gate, up, down, whole, parcel, shared):
     blocks = []
     for t in range(got.shape[0]):
         for j in range(got.shape[2] // LANES):
@@ -271,9 +283,13 @@
     whole[...] = normed
     picked = jnp.dot(dispatch[:, 0:GROUP], normed, preferred_element_type=jnp.float32)
     parcel[...] = picked.astype(jnp.bfloat16).reshape(parcel.shape)
-
-
-def normalize_and_pick(got, dispatch, rows):
+    gated = jnp.dot(normed, gate[...], preferred_element_type=jnp.float32)
+    upped = jnp.dot(normed, up[...], preferred_element_type=jnp.float32)
+    inner = (gated / (1.0 + jnp.exp(-gated)) * upped).astype(jnp.bfloat16)
+    shared[...] = jnp.dot(inner, down[...], preferred_element_type=jnp.float32)
+
+
+def normalize_and_pick(got, dispatch, gate, up, down, rows):
     wide = got.shape[0] * got.shape[2]
     vector = pl.BlockSpec(memory_space=pltpu.VMEM)
     return pl.pallas_call(
@@ -281,12 +297,13 @@
         out_shape=(
             jax.ShapeDtypeStruct((GROUP, wide), jnp.bfloat16),
             jax.ShapeDtypeStruct((dispatch.shape[0] * wide // LANES, LANES), jnp.bfloat16),
+            jax.ShapeDtypeStruct((GROUP, wide), jnp.float32),
         ),
-        in_specs=[vector] * 2,
-        out_specs=(vector, vector),
+        in_specs=[vector] * 5,
+        out_specs=(vector,) * 3,
         compiler_params=GRANT,
         name="norm",
-    )(got, dispatch)
+    )(got, dispatch, gate, up, down)
 
 
 def expert_kernel(rows, packed, side, out):
@@ -426,14 +443,10 @@
             swaps.append((e * peers + t, e * peers + partner % peers))
     side = lax.ppermute(packed, ("ep", "tp"), swaps)
 
-    whole, parcel = normalize_and_pick(got, dispatch, rows)
+    whole, parcel, shared = normalize_and_pick(
+        got, dispatch, shared_gate, shared_up, shared_down, rows
+    )
     arrived = exchanged(parcel.reshape(experts, blocks, LANES), "ep")
-    shared_hidden = (
-        jax.nn.silu(jnp.dot(whole, shared_gate, preferred_element_type=jnp.float32))
-        * jnp.dot(whole, shared_up, preferred_element_type=jnp.float32)
-    ).astype(jnp.bfloat16)
-    shared = jnp.dot(shared_hidden, shared_down, preferred_element_type=jnp.float32)
-    side, shared = lax.optimization_barrier((side, shared))
     produced = run_expert(arrived.reshape(experts * blocks, LANES), packed, side)
     returned = exchanged(produced.reshape(experts, blocks, LANES), "ep")
     partial = combine_parts(

time: 93.6 us -> 92.2 us (0.985)
  blocking collectives: 46 us -> 80.8 us
  starting transfers between devices: 25.1 us -> 5.2 us
  waiting for transfers between devices: 14.8 us -> 0.01 us
  Pallas kernels: 6.75 us -> 5.75 us
    all_to_all x4 -> x5, blocking collectives: 46 us -> 80.8 us  [exchanged(): return lax.all_to_all(blocks, axis, split_axis=0, concat_axis=0, tiled=True)]
    all_to_all x1 -> x0, starting transfers between devices: 19.8 us -> none  [exchanged(): return lax.all_to_all(blocks, axis, split_axis=0, concat_axis=0, tiled=True)]
    all_to_all x1 -> x0, waiting for transfers between devices: 14.8 us -> none  [exchanged(): return lax.all_to_all(blocks, axis, split_axis=0, concat_axis=0, tiled=True)]
  transfers between devices with their start and end apart: 2 -> 1, of which waited for: 1 -> 0; matrix products, arithmetic and copies ran while one was open for 0% -> 0% of each run, Pallas kernels for 1% -> 1%
where the time goes in v6:
time: 92.2 us; the launch traced here: 91.9 us
  blocking collectives  80.8 us (88%)
  Pallas kernels  5.75 us (6%)
  starting transfers between devices  5.2 us (6%)
    all_to_all x5, blocking collectives, exchanged(): return lax.all_to_all(blocks, axis, split_axis=0, concat_axis=0, tiled=True)  80.8 us
    ppermute x1, starting transfers between devices, body(): side = lax.ppermute(packed, ('ep', 'tp'), swaps)  5.2 us
    pallas_call x1, Pallas kernels, stick_read(): pl.pallas_call(stick_kernel, out_shape=(jax.ShapeDtypeStruct((copies, PAD...  3.44 us
  transfers between devices with their start and end apart: 1, of which 0 were waited for; matrix products, arithmetic and copies ran while one was open for 0% of the time, Pallas kernels for 1%

profile of v6, /device:TPU:1, one launch (start us, length us, event | category | flops | bytes accessed | tf_op | source)
XLA Modules:
  0.0 91.9 jit_solution(8469586688915450160)
XLA Ops:
  0.0 0.0 copy-start.3
  0.0 0.0 copy-start.4
  0.0 0.0 copy-start.5
  0.0 0.0 copy-start.6
  0.0 0.0 copy-start
  0.0 0.0 copy-start.1
  0.0 0.0 copy-start.2
  0.0 3.4 %stick.1 = (bf16[4,8,512]{2,1,0:T(8,128)(2,1)S(1)}, bf16[3072,128]{1,0:T(8,128)(2,1)S(1)}, bf16[128,128]{1,0:T(8,128)(2,1)S(1)}, bf16[24,128]{1,0:T(8,128)(2,1)S(1)}, bf16[24,128]{1,0:T(8,128)(2,1)S(1)}) custom-call(s32[5]{0:T(128)} %lengths_at.1, f32[8]{0:T(128)} %offsets_at.1, bf16[5,512]{1,0:T(8,128)(2,1)} %queries_at.1, s32[6,20]{1,0:T(8,128)} %bitcast.20, ...), custom_call_target="tpu_custom_call" | custom-call | tf_op jit(solution)/shard_map/stick/pallas_call | solution.py:187
  3.5 5.2 %collective-permute-start = (bf16[3072,128]{1,0:T(8,128)(2,1)S(1)}, bf16[3072,128]{1,0:T(8,128)(2,1)S(1)}, u32[]{:S(2)}, u32[]{:S(2)}) collective-permute-start(bf16[3072,128]{1,0:T(8,128)(2,1)S(1)} %get-tuple-element.18.packed), channel_id=1, source_target_pairs={{0,1},{1,0},{2,3},{3,2},{4,7},{5,6},{6,5},{7,4},{8,9},{9,8},{10,11... | collective-permute-start | bytes 2359304 | tf_op jit(solution)/shard_map/ppermute | solution.py:444
  8.7 9.5 %all_to_all.25 = bf16[4,8,512]{2,1,0:T(8,128)(2,1)S(1)} all-to-all(bf16[4,8,512]{2,1,0:T(8,128)(2,1)S(1)} %get-tuple-element.15), channel_id=1, replica_groups=mesh['ep'=128,'tp'=4] {'tp'}, dimensions={0} | all-to-all | bytes 65536 | tf_op jit(solution)/shard_map/all_to_all | solution.py:401
  18.3 0.0 copy-done.3
  18.3 0.0 copy-done.4
  18.3 0.0 copy-done.5
  18.3 0.0 copy-done.6
  18.3 0.2 project.1
  18.4 8.5 %all_to_all.26.got = f32[4,24,256]{2,1,0:T(8,128)S(1)} all-to-all(f32[4,24,256]{2,1,0:T(8,128)S(1)} %project.1), channel_id=1, replica_groups=mesh['ep'=128,'tp'=4] {'tp'}, dimensions={0} | all-to-all | bytes 196608 | tf_op jit(solution)/shard_map/all_to_all | solution.py:401
  26.9 0.0 copy-done
  26.9 0.0 copy-done.1
  26.9 0.0 copy-done.2
  26.9 0.5 norm.1
  27.5 34.8 %all_to_all.27 = bf16[128,8,128]{2,1,0:T(8,128)(2,1)S(1)} all-to-all(bf16[128,8,128]{2,1,0:T(8,128)(2,1)S(1)} %bitcast.14), channel_id=1, replica_groups=mesh['ep'=128,'tp'=4] {'ep'}, dimensions={0} | all-to-all | bytes 524288 | tf_op jit(solution)/shard_map/all_to_all | solution.py:401
  62.3 0.0 collective-permute-done.side
  62.3 0.0 copy-start.7
  62.3 0.0 copy-start.8
  62.3 0.6 expert.1
  62.9 20.2 %all_to_all.28 = bf16[128,8,128]{2,1,0:T(8,128)(2,1)S(1)} all-to-all(bf16[128,8,128]{2,1,0:T(8,128)(2,1)S(1)} %bitcast.13), channel_id=1, replica_groups=mesh['ep'=128,'tp'=4] {'ep'}, dimensions={0} | all-to-all | bytes 524288 | tf_op jit(solution)/shard_map/all_to_all | solution.py:401
  83.2 0.3 combine.1
  83.4 7.8 %all_to_all.29.partials = bf16[4,24,1024]{2,1,0:T(8,128)(2,1)S(1)} all-to-all(bf16[4,24,1024]{2,1,0:T(8,128)(2,1)S(1)} %combine.1), channel_id=1, replica_groups=mesh['ep'=128,'tp'=4] {'tp'}, dimensions={0} | all-to-all | bytes 393216 | tf_op jit(solution)/shard_map/all_to_all | solution.py:401
  91.2 0.0 copy-done.7
  91.2 0.0 copy-done.8
  91.2 0.7 finish.1
Async XLA Ops:
  0.0 18.3 %copy-start.3 = (bf16[512,256]{1,0:T(8,128)(2,1)S(1)}, bf16[512,256]{1,0:T(8,128)(2,1)}, u32[]{:S(2)}) copy-start(bf16[512,256]{1,0:T(8,128)(2,1)} %weight.1) | copy-start | bytes 786436
  0.0 18.3 %copy-start.4 = (bf16[20,256]{1,0:T(8,128)(2,1)S(1)}, bf16[20,256]{1,0:T(8,128)(2,1)}, u32[]{:S(2)}) copy-start(bf16[20,256]{1,0:T(8,128)(2,1)} %residual.1) | copy-start | bytes 30724
  0.0 18.3 %copy-start.5 = (f32[256]{0:T(256)S(1)}, f32[256]{0:T(256)}, u32[]{:S(2)}) copy-start(f32[256]{0:T(256)} %param.26) | copy-start | bytes 3076
  0.0 18.3 %copy-start.6 = (f32[256]{0:T(256)S(1)}, f32[256]{0:T(256)}, u32[]{:S(2)}) copy-start(f32[256]{0:T(256)} %param.27) | copy-start | bytes 3076
  0.0 26.9 %copy-start = (bf16[1024,128]{1,0:T(8,128)(2,1)S(1)}, bf16[1024,128]{1,0:T(8,128)(2,1)}, u32[]{:S(2)}) copy-start(bf16[1024,128]{1,0:T(8,128)(2,1)} %gate.3) | copy-start | bytes 786436
  0.0 26.9 %copy-start.1 = (bf16[1024,128]{1,0:T(8,128)(2,1)S(1)}, bf16[1024,128]{1,0:T(8,128)(2,1)}, u32[]{:S(2)}) copy-start(bf16[1024,128]{1,0:T(8,128)(2,1)} %up.3) | copy-start | bytes 786436
  0.0 26.9 %copy-start.2 = (bf16[128,1024]{1,0:T(8,128)(2,1)S(1)}, bf16[128,1024]{1,0:T(8,128)(2,1)}, u32[]{:S(2)}) copy-start(bf16[128,1024]{1,0:T(8,128)(2,1)} %down.3) | copy-start | bytes 786436
  3.5 58.8 %collective-permute-start = (bf16[3072,128]{1,0:T(8,128)(2,1)S(1)}, bf16[3072,128]{1,0:T(8,128)(2,1)S(1)}, u32[]{:S(2)}, u32[]{:S(2)}) collective-permute-start(bf16[3072,128]{1,0:T(8,128)(2,1)S(1)} %get-tuple-element.18.packed), channel_id=1, source_target_pairs={{0,1},{1,0},{2,3},{3,2},{4,7},{5,6},{6,5},{7,4},{8,9},{9,8},{10,11... | collective-permute-start | bytes 2359304 | tf_op jit(solution)/shard_map/ppermute | solution.py:444
  62.3 28.9 %copy-start.7 = (f32[256]{0:T(256)S(1)}, f32[256]{0:T(256)}, u32[]{:S(2)}) copy-start(f32[256]{0:T(256)} %param.36) | copy-start | bytes 3076
  62.3 28.9 %copy-start.8 = (f32[256]{0:T(256)S(1)}, f32[256]{0:T(256)}, u32[]{:S(2)}) copy-start(f32[256]{0:T(256)} %param.37) | copy-start | bytes 3076
